TPU v7x, 512 devices: a 8x2x16 block of a 8x16x16 slice. The times are simulated.
512 devices in a mesh: grp: 2 (over y), ra: 16 (over z), cb: 16 (over x, core).
Axes of the slice: x: 8, y: 2, z: 16, core: 2. Of those that a mesh axis runs over, the one named last changes fastest.
The devices are a block of a 8x16x16 slice.
Arguments:
- tokens: bfloat16 [256, 4096], P('grp', 'ra'), parts along dimension 0, may hold values from -20 to 20
- norm_gain: float32 [4096], P('ra'), may hold values from 0.1 to 1.9
- gate_weight: float32 [4096, 11264], P('ra', 'cb'), may hold values from -0.09375 to 0.09375
- gate_scale: float32 [11264], P('cb'), may hold values from 0.5 to 2
- up_weight: float32 [4096, 11264], P('ra', 'cb'), may hold values from -0.09375 to 0.09375
- up_scale: float32 [11264], P('cb'), may hold values from 0.5 to 2
- down_weight: float32 [11264, 4096], P('cb', 'ra'), may hold values from -1 to 1
- down_scale: float32 [4096], P('ra'), may hold values from 0.5 to 2
- out_gain: float32 [4096], P('ra'), may hold values from 0.1 to 1.9
Outputs:
- normed: bfloat16 [256, 4096], P('grp', 'ra'), parts along dimension 0
There are 2 independent parts, one for each index of `grp`. A program takes and returns all parts, laid end to end along the dimension named above; an argument that names none is the same for every part. Nothing has to cross between parts.
All inputs are finite; a program needn't handle non-finite values.
Results may differ from a plain program's by a relative error of at most 0.012.
Values may be sent and summed in bfloat16 or wider, within the bound.
A program may use at most 64 MiB of HBM per device.

v0:
```python
import jax
import jax.numpy as jnp
from jax import lax
from jax.sharding import PartitionSpec as P


def copy_for_each(value, axis):
    size = lax.axis_size(axis)
    return lax.all_to_all(
        jnp.broadcast_to(value[None], (size, *value.shape)), axis, 0, 0, tiled=True
    )


def over_copies(value, axis):
    everything = copy_for_each(value, axis)
    return jnp.sum(everything, axis=0)


def in_blocks(value, dim, size):
    shape = value.shape
    tiles = value.reshape(*shape[:dim], size, shape[dim] // size, *shape[dim + 1 :])
    return jnp.moveaxis(tiles, dim, 0)


def summed_on_arrival(value, axis, dim):
    size = lax.axis_size(axis)
    tiles = lax.all_to_all(in_blocks(value, dim, size), axis, 0, 0, tiled=True)
    return jnp.sum(tiles.astype(jnp.float32), axis=0)


def side_by_side(arrays, axis, dim, along):
    widths = [a.shape[along] for a in arrays]
    both = jnp.concatenate(arrays, axis=along)
    filled = summed_on_arrival(both, axis, dim)
    return tuple(jnp.split(filled, [sum(widths[:k]) for k in range(1, len(widths))], axis=along))


def laid_out(tiles, dim):
    shape = list(tiles.shape[1:])
    shape[dim] *= tiles.shape[0]
    return jnp.moveaxis(tiles, 0, dim).reshape(shape)


def collect(value, axis, dim):
    tiles = copy_for_each(value, axis)
    return laid_out(tiles, dim)


def of_everyone(value, axis):
    everything = copy_for_each(value, axis)
    return jnp.sum(everything.astype(jnp.float32), axis=0)


def on_device(
    tokens,
    norm_gain,
    gate_weight,
    gate_scale,
    up_weight,
    up_scale,
    down_weight,
    down_scale,
    out_gain,
):
    width = tokens.shape[1] * lax.axis_size("ra")
    values = tokens.astype(jnp.float32)
    squares = over_copies(jnp.sum(values * values, axis=1), "ra")
    inv_first = lax.rsqrt(squares / width + 1e-06)[:, None]
    normed_in = (values * inv_first * norm_gain).astype(jnp.bfloat16)
    gate_local = gate_weight.astype(jnp.bfloat16)
    up_local = up_weight.astype(jnp.bfloat16)
    down_local = down_weight.astype(jnp.bfloat16)
    gate_part = jnp.dot(normed_in, gate_local, preferred_element_type=jnp.float32)
    up_part = jnp.dot(normed_in, up_local, preferred_element_type=jnp.float32)
    gate, up = side_by_side(
        (gate_part.astype(jnp.bfloat16), up_part.astype(jnp.bfloat16)), "ra", 1, 0
    )
    share = gate.shape[1]
    offset = lax.axis_index("ra") * share
    gate_cols = lax.dynamic_slice_in_dim(gate_scale, offset, share, 0)
    up_cols = lax.dynamic_slice_in_dim(up_scale, offset, share, 0)
    hidden_share = (jax.nn.silu(gate * gate_cols) * (up * up_cols)).astype(jnp.bfloat16)
    partial_value = jnp.dot(
        collect(hidden_share, "ra", 1), down_local, preferred_element_type=jnp.float32
    )
    branch = of_everyone(partial_value.astype(jnp.bfloat16), "cb").astype(jnp.float32) * down_scale
    mixed = 0.5 * values + branch
    second = over_copies(jnp.sum(mixed * mixed, axis=1), "ra")
    inv_second = lax.rsqrt(second / width + 1e-06)[:, None]
    return (mixed * inv_second * out_gain).astype(jnp.bfloat16)


def solution(mesh):
    return jax.shard_map(
        on_device,
        mesh=mesh,
        in_specs=(
            P("grp", "ra"),
            P("ra"),
            P("ra", "cb"),
            P("cb"),
            P("ra", "cb"),
            P("cb"),
            P("cb", "ra"),
            P("ra"),
            P("ra"),
        ),
        out_specs=P("grp", "ra"),
        check_vma=False,
    )
```

profile of v0, /device:TPU:65, one launch (start us, length us, event | category | flops | bytes accessed | tf_op | source)
XLA Modules:
  0.0 162.5 jit_solution(8770880777833187907)
XLA Ops:
  0.0 1.0 fusion.4
  1.0 55.1 %all_to_all.27 = f32[16,1,128]{2,1,0:T(1,128)S(1)} all-to-all(f32[16,1,128]{2,1,0:T(1,128)S(1)} %broadcast_in_dim.8), channel_id=1, replica_groups=mesh['grp'=2,'ra'=16,'cb'=16] {'ra'}, dimensions={0} | all-to-all | bytes 16384 | tf_op jit(solution)/shard_map/all_to_all | solution.py:9
  56.2 1.5 convolution_convert_fusion
  57.7 0.0 copy-done
  57.7 0.0 copy-done.4
  57.7 0.0 copy-done.1
  57.7 0.3 convolution_convert_fusion.1
  58.1 0.8 reshape.35
  58.9 4.1 %all-to-all-start.1 = ((bf16[16,256,44]{1,2,0:T(8,128)(2,1)}), bf16[16,256,44]{1,2,0:T(8,128)(2,1)S(1)}, u32[]{:S(2)}, u32[]{:S(2)}) async-start(bf16[16,256,44]{1,2,0:T(8,128)(2,1)} %bitcast.1), calls=%async_computation.1 | async-start | bytes 786432 | tf_op jit(solution)/shard_map/all_to_all | solution.py:27
  63.1 0.8 dynamic_slice.6
  63.8 0.8 dynamic_slice.7
  64.6 16.3 %all-to-all-done.1 = bf16[16,256,44]{1,2,0:T(8,128)(2,1)S(1)} async-done(((bf16[16,256,44]{1,2,0:T(8,128)(2,1)}), bf16[16,256,44]{1,2,0:T(8,128)(2,1)S(1)}, u32[]{:S(2)}, u32[]{:S(2)}) %all-to-all-start.1) | async-done | bytes 360480 | tf_op jit(solution)/shard_map/all_to_all | solution.py:27
  80.9 0.1 convert_reduce_fusion.1
  80.9 0.1 fusion.8
  81.1 23.1 %all_to_all.28 = bf16[16,128,44]{1,2,0:T(8,128)(2,1)S(1)} all-to-all(bf16[16,128,44]{1,2,0:T(8,128)(2,1)S(1)} %broadcast_in_dim.9), channel_id=1, replica_groups=mesh['grp'=2,'ra'=16,'cb'=16] {'ra'}, dimensions={0} | all-to-all | bytes 360448 | tf_op jit(solution)/shard_map/all_to_all | solution.py:9
  104.2 0.0 copy-done.2
  104.2 0.3 convolution_convert_fusion.2
  104.4 0.1 broadcast_in_dim.10
  104.5 40.8 %all_to_all.29 = bf16[16,128,256]{2,1,0:T(8,128)(2,1)S(1)} all-to-all(bf16[16,128,256]{2,1,0:T(8,128)(2,1)S(1)} %broadcast_in_dim.10), channel_id=1, replica_groups=mesh['grp'=2,'ra'=16,'cb'=16] {'cb'}, dimensions={0} | all-to-all | bytes 2097152 | tf_op jit(solution)/shard_map/all_to_all | solution.py:9
  145.3 0.1 convert_reduce_fusion
  145.5 0.5 copy-done.3
  146.0 0.1 multiply_reduce_fusion
  146.1 15.6 %all_to_all.30 = f32[16,1,128]{2,1,0:T(1,128)S(1)} all-to-all(f32[16,1,128]{2,1,0:T(1,128)S(1)} %broadcast_in_dim.11), channel_id=1, replica_groups=mesh['grp'=2,'ra'=16,'cb'=16] {'ra'}, dimensions={0} | all-to-all | bytes 16384 | tf_op jit(solution)/shard_map/all_to_all | solution.py:9
  161.7 0.7 multiply_convert_fusion
  (16 shorter events, 0.2 us)
Async XLA Ops:
  0.0 57.7 %copy-start = (bf16[128,256]{1,0:T(8,128)(2,1)S(1)}, bf16[128,256]{1,0:T(8,128)(2,1)}, u32[]{:S(2)}) copy-start(bf16[128,256]{1,0:T(8,128)(2,1)} %param.9) | copy-start | bytes 196612
  0.0 57.7 %copy-start.4 = (f32[256]{0:T(256)S(1)}, f32[256]{0:T(256)}, u32[]{:S(2)}) copy-start(f32[256]{0:T(256)} %param.10) | copy-start | bytes 3076
  0.0 57.7 %copy-start.1 = (f32[256,704]{0,1:T(8,128)S(1)}, f32[256,704]{0,1:T(8,128)}, u32[]{:S(2)}) copy-start(f32[256,704]{0,1:T(8,128)} %param.11) | copy-start | bytes 2162692
  58.9 45.2 %copy-start.2 = (f32[704,256]{1,0:T(8,128)S(1)}, f32[704,256]{1,0:T(8,128)}, u32[]{:S(2)}) copy-start(f32[704,256]{1,0:T(8,128)} %param.15) | copy-start | bytes 2162692
  58.9 21.9 %all-to-all-start.1 = ((bf16[16,256,44]{1,2,0:T(8,128)(2,1)}), bf16[16,256,44]{1,2,0:T(8,128)(2,1)S(1)}, u32[]{:S(2)}, u32[]{:S(2)}) async-start(bf16[16,256,44]{1,2,0:T(8,128)(2,1)} %bitcast.1), calls=%async_computation.1 | async-start | bytes 786432 | tf_op jit(solution)/shard_map/all_to_all | solution.py:27
  145.3 0.7 copy-start.3
  145.3 16.4 %copy-start.5 = (f32[256]{0:T(256)S(1)}, f32[256]{0:T(256)}, u32[]{:S(2)}) copy-start(f32[256]{0:T(256)} %param.17) | copy-start | bytes 3076
where the time goes:
time: 163 us; the launch traced here: 162 us
  blocking collectives  135 us (83%)
  waiting for transfers between devices  16.3 us (10%)
  starting transfers between devices  4.12 us (3%)
  local copies, waits for them, and re-layouts  3.05 us (2%)
  other arithmetic  2.23 us (1%)
  matrix products  2.07 us (1%)
    all_to_all x4, blocking collectives, copy_for_each(): lax.all_to_all(jnp.broadcast_to(value[None], (size, *value.shape)), axis,...  135 us
    all_to_all x1, waiting for transfers between devices, summed_on_arrival(): tiles = lax.all_to_all(in_blocks(value, dim, size), axis, 0, 0, tiled=True)  16.3 us
    all_to_all x1, starting transfers between devices, summed_on_arrival(): tiles = lax.all_to_all(in_blocks(value, dim, size), axis, 0, 0, tiled=True)  4.12 us
  transfers between devices with their start and end apart: 1, of which 1 were waited for; matrix products, arithmetic and copies ran while one was open for 1% of the time, Pallas kernels for 0%

commit v1 on v0

v1 whole, which is shorter than its diff:
```python
import functools

import jax
import jax.numpy as jnp
from jax import lax
from jax.experimental import pallas as pl
from jax.experimental.pallas import tpu as pltpu
from jax.sharding import PartitionSpec as P

MESH = pl.DeviceIdType.MESH
LANES = 128
F32 = jnp.float32
BF16 = jnp.bfloat16


def far_first(n):
    return sorted(range(1, n), key=lambda d: -min(d, n - d))


def kernel(
    nz,
    nc,
    tok_ref,
    gain_ref,
    gw_ref,
    gs_ref,
    uw_ref,
    us_ref,
    dw_ref,
    ds_ref,
    og_ref,
    out_ref,
    gw_v,
    uw_v,
    dw_v,
    part,
    got,
    hid,
    pair,
    pair_got,
    chips,
    squares,
    load_sem,
    rs_send,
    rs_recv,
    ag_send,
    ag_recv,
    pr_send,
    pr_recv,
    x_send,
    x_recv,
    sq_send,
    sq_recv,
    o_send,
    o_recv,
):
    z = lax.axis_index("ra")
    cb = lax.axis_index("cb")
    chip = cb // 2
    core = cb % 2
    nx = nc // 2
    tokens, feats = tok_ref.shape
    units = gw_ref.shape[1]
    main = units // LANES * LANES
    rest = units - main
    tile = tokens // nz
    half = tokens // 2
    width = feats * nz

    loads = [
        pltpu.make_async_copy(src, dst, load_sem.at[k])
        for k, (src, dst) in enumerate([(gw_ref, gw_v), (uw_ref, uw_v), (dw_ref, dw_v.at[:units])])
    ]
    for copy in loads:
        copy.start()

    def to_z(d):
        return {"ra": lax.rem(z + d, nz)}

    def to_chip(d):
        return {"cb": lax.rem(chip + d, nx) * 2 + core}

    mate = {"cb": chip * 2 + 1 - core}

    barrier = pltpu.get_barrier_semaphore()
    peers = [to_z(d) for d in range(1, nz)] + [to_chip(d) for d in range(1, nx)] + [mate]
    for peer in peers:
        pl.semaphore_signal(barrier, inc=1, device_id=peer, device_id_type=MESH)

    values = tok_ref[...].astype(F32)
    scaled = (values * gain_ref[...]).astype(BF16)
    own_squares = jnp.sum(values * values, axis=1, keepdims=True)
    lane = lax.broadcasted_iota(jnp.int32, (tokens, LANES), 1)
    high = own_squares.astype(BF16).astype(F32)
    low = own_squares - high
    tail = jnp.where(lane == 0, high, jnp.where(lane == 1, low, 0.0))

    def put(columns, value):
        part[:, :, columns] = value.reshape(nz, tile, value.shape[1]).astype(BF16)

    put(slice(2 * main + 2 * rest, 2 * main + 2 * rest + LANES), tail)
    loads[0].wait()
    gate = jnp.dot(scaled, gw_v[...].astype(BF16), preferred_element_type=F32)
    put(slice(0, main), gate[:, :main])
    loads[1].wait()
    up = jnp.dot(scaled, uw_v[...].astype(BF16), preferred_element_type=F32)
    put(slice(main, 2 * main), up[:, :main])
    put(
        slice(2 * main, 2 * main + 2 * rest),
        jnp.concatenate([gate[:, main:], up[:, main:]], axis=1),
    )

    pl.semaphore_wait(barrier, len(peers))

    sends = []
    for d in far_first(nz):
        copy = pltpu.make_async_remote_copy(
            src_ref=part.at[lax.rem(z + d, nz)],
            dst_ref=got.at[d - 1],
            send_sem=rs_send.at[d - 1],
            recv_sem=rs_recv.at[d - 1],
            device_id=to_z(d),
            device_id_type=MESH,
        )
        copy.start()
        sends.append((d, copy))

    loads[2].wait()
    down = dw_v[...]
    pad = dw_v.shape[0] - units
    down = jnp.where(lax.broadcasted_iota(jnp.int32, down.shape, 0) < units, down, 0.0).astype(BF16)

    total = part[z].astype(F32)
    for d, copy in reversed(sends):
        copy.wait_recv()
        total += got[d - 1].astype(F32)
    square = jnp.sum(total[:, 2 * main + 2 * rest :], axis=1, keepdims=True)
    inv = lax.rsqrt(square / width + 1e-06)
    gate_scale = gs_ref[...]
    up_scale = us_ref[...]
    g = total[:, :main] * inv * gate_scale[:, :main]
    u = total[:, main : 2 * main] * inv * up_scale[:, :main]
    mixed_scale = jnp.concatenate([gate_scale[:, main:], up_scale[:, main:]], axis=1)
    both = total[:, 2 * main : 2 * main + 2 * rest] * inv * mixed_scale
    swapped = pltpu.roll(both, rest, 1)
    hid[z, :, :main] = (g * jax.nn.sigmoid(g) * u).astype(BF16)
    last = both * jax.nn.sigmoid(both) * swapped
    last_lane = lax.broadcasted_iota(jnp.int32, last.shape, 1)
    hid[z, :, main:] = jnp.where(last_lane < rest, last, 0.0).astype(BF16)

    hid_sends = []
    for d in far_first(nz):
        copy = pltpu.make_async_remote_copy(
            src_ref=hid.at[z],
            dst_ref=hid.at[z],
            send_sem=ag_send.at[d - 1],
            recv_sem=ag_recv.at[d - 1],
            device_id=to_z(d),
            device_id_type=MESH,
        )
        copy.start()
        hid_sends.append(copy)
    for d in far_first(nz):
        pltpu.make_async_remote_copy(
            src_ref=hid.at[z],
            dst_ref=hid.at[lax.rem(z + nz - d, nz)],
            send_sem=ag_send.at[d - 1],
            recv_sem=ag_recv.at[d - 1],
            device_id=to_z(d),
            device_id_type=MESH,
        ).wait_recv()

    partial = jnp.dot(
        hid[...].reshape(tokens, hid.shape[2]), down, preferred_element_type=F32
    )
    pair[0] = partial[:half].astype(BF16)
    pair[1] = partial[half:].astype(BF16)
    pair_copy = pltpu.make_async_remote_copy(
        src_ref=pair.at[1 - core],
        dst_ref=pair_got,
        send_sem=pr_send,
        recv_sem=pr_recv,
        device_id=mate,
        device_id_type=MESH,
    )
    pair_copy.start()
    pair_copy.wait_recv()
    chips[chip] = (pair[core].astype(F32) + pair_got[...].astype(F32)).astype(BF16)

    x_sends = []
    for d in far_first(nx):
        copy = pltpu.make_async_remote_copy(
            src_ref=chips.at[chip],
            dst_ref=chips.at[chip],
            send_sem=x_send.at[d - 1],
            recv_sem=x_recv.at[d - 1],
            device_id=to_chip(d),
            device_id_type=MESH,
        )
        copy.start()
        x_sends.append(copy)
    for d in far_first(nx):
        pltpu.make_async_remote_copy(
            src_ref=chips.at[chip],
            dst_ref=chips.at[lax.rem(chip + nx - d, nx)],
            send_sem=x_send.at[d - 1],
            recv_sem=x_recv.at[d - 1],
            device_id=to_chip(d),
            device_id_type=MESH,
        ).wait_recv()

    branch = chips[0].astype(F32)
    for k in range(1, nx):
        branch += chips[k].astype(F32)
    rows = pl.ds(pl.multiple_of(core * half, half), half)
    mixed = 0.5 * tok_ref[rows, :].astype(F32) + branch * ds_ref[...]
    column = jnp.sum(mixed * mixed, axis=1, keepdims=True)
    diagonal = lax.broadcasted_iota(jnp.int32, (half, LANES), 0) == lax.broadcasted_iota(
        jnp.int32, (half, LANES), 1
    )
    squares[z] = jnp.sum(jnp.where(diagonal, column, 0.0), axis=0, keepdims=True)

    sq_sends = []
    for d in far_first(nz):
        copy = pltpu.make_async_remote_copy(
            src_ref=squares.at[z],
            dst_ref=squares.at[z],
            send_sem=sq_send.at[d - 1],
            recv_sem=sq_recv.at[d - 1],
            device_id=to_z(d),
            device_id_type=MESH,
        )
        copy.start()
        sq_sends.append(copy)
    for d in far_first(nz):
        pltpu.make_async_remote_copy(
            src_ref=squares.at[z],
            dst_ref=squares.at[lax.rem(z + nz - d, nz)],
            send_sem=sq_send.at[d - 1],
            recv_sem=sq_recv.at[d - 1],
            device_id=to_z(d),
            device_id_type=MESH,
        ).wait_recv()
    everything = squares[0]
    for k in range(1, nz):
        everything += squares[k]
    inv_row = lax.rsqrt(everything / width + 1e-06)
    inv_second = jnp.sum(jnp.where(diagonal, inv_row, 0.0), axis=1, keepdims=True)
    out_ref[rows, :] = (mixed * inv_second * og_ref[...]).astype(BF16)
    out_copy = pltpu.make_async_remote_copy(
        src_ref=out_ref.at[rows],
        dst_ref=out_ref.at[rows],
        send_sem=o_send,
        recv_sem=o_recv,
        device_id=mate,
        device_id_type=MESH,
    )
    out_copy.start()
    for _, copy in sends:
        copy.wait_send()
    for copy in hid_sends + [pair_copy] + x_sends + sq_sends:
        copy.wait_send()
    out_copy.wait_send()
    other = pl.ds(pl.multiple_of((1 - core) * half, half), half)
    pltpu.make_async_remote_copy(
        src_ref=out_ref.at[other],
        dst_ref=out_ref.at[other],
        send_sem=o_send,
        recv_sem=o_recv,
        device_id=mate,
        device_id_type=MESH,
    ).wait_recv()


def solution(mesh):
    nz, nc = mesh.shape["ra"], mesh.shape["cb"]

    def on_device(tokens, norm_gain, gw, gs, uw, us, dw, ds, og):
        count, feats = tokens.shape
        units = gw.shape[1]
        padded = -(-units // LANES) * LANES
        tile = count // nz
        half = count // 2
        vmem = pl.BlockSpec(memory_space=pltpu.VMEM)
        hbm = pl.BlockSpec(memory_space=pl.ANY)
        dma = pltpu.SemaphoreType.DMA
        row = lambda v: v.reshape(1, -1)
        return pl.pallas_call(
            functools.partial(kernel, nz, nc),
            out_shape=jax.ShapeDtypeStruct((count, feats), BF16),
            in_specs=[vmem, vmem, hbm, vmem, hbm, vmem, hbm, vmem, vmem],
            out_specs=vmem,
            scratch_shapes=[
                pltpu.VMEM((feats, units), F32),
                pltpu.VMEM((feats, units), F32),
                pltpu.VMEM((padded, feats), F32),
                pltpu.VMEM((nz, tile, 2 * units + LANES), BF16),
                pltpu.VMEM((nz - 1, tile, 2 * units + LANES), BF16),
                pltpu.VMEM((nz, tile, padded), BF16),
                pltpu.VMEM((2, half, feats), BF16),
                pltpu.VMEM((half, feats), BF16),
                pltpu.VMEM((nc // 2, half, feats), BF16),
                pltpu.VMEM((nz, 1, LANES), F32),
                dma((3,)),
                dma((nz - 1,)),
                dma((nz - 1,)),
                dma((nz - 1,)),
                dma((nz - 1,)),
                dma,
                dma,
                dma((nc // 2 - 1,)),
                dma((nc // 2 - 1,)),
                dma((nz - 1,)),
                dma((nz - 1,)),
                dma,
                dma,
            ],
            compiler_params=pltpu.CompilerParams(collective_id=0, has_side_effects=True),
        )(tokens, row(norm_gain), gw, row(gs), uw, row(us), dw, row(ds), row(og))

    return jax.shard_map(
        on_device,
        mesh=mesh,
        in_specs=(
            P("grp", "ra"),
            P("ra"),
            P("ra", "cb"),
            P("cb"),
            P("ra", "cb"),
            P("cb"),
            P("cb", "ra"),
            P("ra"),
            P("ra"),
        ),
        out_specs=P("grp", "ra"),
        check_vma=False,
    )
```

time: 163 us -> 106 us (0.65)
  blocking collectives: 135 us -> 0 us
  Pallas kernels: 0 us -> 99.1 us
  waiting for transfers between devices: 16.3 us -> 0 us
  starting transfers between devices: 4.12 us -> 0 us
  local copies, waits for them, and re-layouts: 3.05 us -> 6.85 us
  other arithmetic: 2.23 us -> 0 us
  matrix products: 2.07 us -> 0 us
    all_to_all x4 -> x0, blocking collectives: 135 us -> none  [copy_for_each(): lax.all_to_all(jnp.broadcast_to(value[None], (size, *value.shape)), axis,...]
    pallas_call x0 -> x1, Pallas kernels: none -> 99.1 us  [on_device(): pl.pallas_call(functools.partial(kernel, nz, nc), out_shape=jax.ShapeDtyp...]
    all_to_all x1 -> x0, waiting for transfers between devices: 16.3 us -> none  [summed_on_arrival(): tiles = lax.all_to_all(in_blocks(value, dim, size), axis, 0, 0, tiled=True)]
    unnamed x12 -> x9, local copies, waits for them, and re-layouts: 0.55 us -> 5.68 us
    all_to_all x1 -> x0, starting transfers between devices: 4.12 us -> none  [summed_on_arrival(): tiles = lax.all_to_all(in_blocks(value, dim, size), axis, 0, 0, tiled=True)]
    dot_general x3 -> x0, matrix products: 2.07 us -> none  [the longest x1 1.48 us: on_device(): up_part = jnp.dot(normed_in, up_local, preferred_element_type=jnp.float32)]
  transfers between devices with their start and end apart: 1 -> 0, of which waited for: 1 -> 0; matrix products, arithmetic and copies ran while one was open for 1% -> 0% of each run, Pallas kernels for 0% -> 0%
where the time goes in v1:
time: 106 us
  Pallas kernels  99.1 us (93%)
  local copies, waits for them, and re-layouts  6.85 us (6%)
    pallas_call x1, Pallas kernels, on_device(): pl.pallas_call(functools.partial(kernel, nz, nc), out_shape=jax.ShapeDtyp...  99.1 us
    unnamed x9, local copies, waits for them, and re-layouts  5.68 us

profile of v1, /device:TPU:65, one launch (start us, length us, event | category | flops | bytes accessed | tf_op | source)
XLA Modules:
  0.0 105.9 jit_solution(7017767104614371387)
XLA Ops:
  0.0 0.0 copy-start.1
  0.0 0.0 copy-start.2
  0.0 0.7 copy-done.1
  0.7 0.6 reshape.16.gs_ref
  1.3 0.0 copy-done.2
  1.3 0.6 reshape.17.us_ref
  1.9 0.0 copy-start
  1.9 2.3 %copy.10.gw_ref = f32[256,704]{1,0:T(8,128)} copy(f32[256,704]{0,1:T(8,128)} %param.11) | data formatting | bytes 1441792 | tf_op args[2]
  4.2 0.0 copy-done
  4.2 1.2 %copy.11.uw_ref = f32[256,704]{1,0:T(8,128)} copy(f32[256,704]{0,1:T(8,128)S(1)} %copy-done) | data formatting | bytes 1441792 | tf_op args[4]
  5.4 99.1 %shard_map.91 = bf16[128,256]{1,0:T(8,128)(2,1)} custom-call(bf16[128,256]{1,0:T(8,128)(2,1)} %tok_ref.1, f32[1,256]{1,0:T(1,128)} %bitcast.3, f32[256,704]{1,0:T(8,128)} %copy.10.gw_ref, f32[1,704]{1,0:T(1,128)} %reshape.16.gs_ref, f32[256,704]{1,0:T(8,128)} %copy.11.uw_ref, f32[1,704]{1,0:T(1,128)} %reshape.17.us_ref, f32[704,256]{1,0:T(8,128)} %dw_ref.1, ...), custom_call_target="tpu_custom_call" | custom-call | tf_op jit(solution)/shard_map/pallas_call | solution.py:288
  104.4 1.5 %copy.13 = bf16[128,256]{1,0:T(8,128)(2,1)} copy(bf16[128,256]{1,0:T(8,128)(2,1)} %shard_map.91) | data formatting | bytes 131072
Async XLA Ops:
  0.0 0.7 copy-start.1
  0.0 1.3 %copy-start.2 = (f32[704]{0:T(1024)S(1)}, f32[704]{0:T(1024)}, u32[]{:S(2)}) copy-start(f32[704]{0:T(1024)} %param.14) | copy-start | bytes 8452
  1.9 2.3 %copy-start = (f32[256,704]{0,1:T(8,128)S(1)}, f32[256,704]{0,1:T(8,128)}, u32[]{:S(2)}) copy-start(f32[256,704]{0,1:T(8,128)} %param.13) | copy-start | bytes 2162692

commit v2 on v0

v2 whole, which is shorter than its diff:
```python
import functools

import jax
import jax.numpy as jnp
from jax import lax
from jax.experimental import pallas as pl
from jax.experimental.pallas import tpu as pltpu
from jax.sharding import PartitionSpec as P

MESH = pl.DeviceIdType.MESH
LANES = 128
F32 = jnp.float32
BF16 = jnp.bfloat16
HOP = 4


def remote(src, dst, send_sem, recv_sem, peer):
    return pltpu.make_async_remote_copy(
        src_ref=src,
        dst_ref=dst,
        send_sem=send_sem,
        recv_sem=recv_sem,
        device_id=peer,
        device_id_type=MESH,
    )


def split_tail(column, lane):
    high = column.astype(BF16).astype(F32)
    return jnp.where(lane == 0, high, jnp.where(lane == 1, column - high, 0.0))


def kernel(
    nz,
    nc,
    tok_ref,
    gain_ref,
    gw_ref,
    gs_ref,
    uw_ref,
    us_ref,
    dw_ref,
    ds_ref,
    og_ref,
    out_ref,
    gu_v,
    dw_v,
    part,
    far_in,
    far_in_half,
    near_in,
    relay_out,
    relay_in,
    hid,
    pair,
    pair_in,
    chips,
    mix,
    squares,
    load_sem,
    far_sems,
    near_sems,
    relay_sems,
    hid_sems,
    pair_sems,
    chip_sems,
    mix_sems,
    sq_sems,
):
    z = lax.axis_index("ra")
    cb = lax.axis_index("cb")
    chip = cb // 2
    core = cb % 2
    nx = nc // 2
    tile, feats = tok_ref.shape[1:]
    tokens = nz * tile
    units = gw_ref.shape[0]
    main = units // LANES * LANES
    rest = units - main
    width = feats * nz
    cols = part.shape[2]
    halves = (slice(0, cols // 2), slice(cols // 2, cols))

    def to_z(d):
        return {"ra": lax.rem(z + d + nz, nz)}

    def to_chip(d):
        return {"cb": lax.rem(chip + d, nx) * 2 + core}

    mate = {"cb": chip * 2 + 1 - core}

    def block(d):
        return lax.rem(z + d + 2 * nz, nz)

    barrier = pltpu.get_barrier_semaphore()
    peers = [to_z(s * d) for d in range(1, HOP + 1) for s in (1, -1)]
    peers += [to_chip(d) for d in range(1, nx)] + [mate]
    for peer in peers:
        pl.semaphore_signal(barrier, inc=1, device_id=peer, device_id_type=MESH)

    loads = [
        pltpu.make_async_copy(src, dst, load_sem.at[k])
        for k, (src, dst) in enumerate(
            [
                (gw_ref.at[:main], gu_v.at[:main]),
                (uw_ref.at[:main], gu_v.at[main : 2 * main]),
                (gw_ref.at[main:], gu_v.at[2 * main : 2 * main + rest]),
                (uw_ref.at[main:], gu_v.at[2 * main + rest :]),
                (dw_ref, dw_v.at[:units]),
            ]
        )
    ]
    for copy in loads:
        copy.start()

    values = tok_ref[...].astype(F32).reshape(tokens, feats)
    scaled = (values * gain_ref[...]).astype(BF16)
    lane = lax.broadcasted_iota(jnp.int32, (tokens, LANES), 1)
    tail = split_tail(jnp.sum(values * values, axis=1, keepdims=True), lane)
    part[:, :, 2 * units :] = tail.reshape(nz, tile, LANES).astype(BF16)
    for copy in loads[:-1]:
        copy.wait()
    both = lax.dot_general(
        scaled, gu_v[...].astype(BF16), (((1,), (1,)), ((), ())), preferred_element_type=F32
    )
    part[:, :, : 2 * units] = both.reshape(nz, tile, 2 * units).astype(BF16)

    pl.semaphore_wait(barrier, len(peers))

    waiting = []
    far = {}
    for k in range(HOP, 0, -1):
        for i, s in enumerate((1, -1)):
            src = part.at[block(s * (k + HOP))]
            dst = far_in.at[i, k - 1] if k < HOP else far_in_half.at[i]
            if k == HOP:
                src = part.at[block(s * (k + HOP)), :, halves[i]]
            far[i, k] = remote(src, dst, far_sems.at[0, i, k - 1], far_sems.at[1, i, k - 1], to_z(s * k))
            far[i, k].start()
    near = {}
    for k in range(HOP - 1, 0, -1):
        for i, s in enumerate((1, -1)):
            near[i, k] = remote(
                part.at[block(s * k)],
                near_in.at[i, k - 1],
                near_sems.at[0, i, k - 1],
                near_sems.at[1, i, k - 1],
                to_z(s * k),
            )
            near[i, k].start()

    loads[-1].wait()
    row = lax.broadcasted_iota(jnp.int32, dw_v.shape, 0)
    down = jnp.where(row < units, dw_v[...], 0.0).astype(BF16)

    tile_lane = lax.broadcasted_iota(jnp.int32, (tile, LANES), 1)
    relay = []
    for i, s in enumerate((1, -1)):
        for k in range(1, HOP + 1):
            far[i, k].wait_recv()
        total = part[block(s * HOP)].astype(F32)
        for k in range(1, HOP):
            total += far_in[i, k - 1].astype(F32)
        half = far_in_half[i].astype(F32)
        pieces = [total[:, halves[0]], total[:, halves[1]]]
        pieces[i] += half
        last = pieces[1][:, -LANES:]
        relay_out[i, :, halves[0]] = pieces[0].astype(BF16)
        relay_out[i, :, cols // 2 : cols - LANES] = pieces[1][:, :-LANES].astype(BF16)
        relay_out[i, :, cols - LANES :] = split_tail(
            jnp.sum(last, axis=1, keepdims=True), tile_lane
        ).astype(BF16)
        copy = remote(
            relay_out.at[i], relay_in.at[i], relay_sems.at[0, i], relay_sems.at[1, i], to_z(s * HOP)
        )
        copy.start()
        relay.append(copy)

    total = part[z].astype(F32)
    for k in range(1, HOP):
        for i in range(2):
            near[i, k].wait_recv()
            total += near_in[i, k - 1].astype(F32)
    gate_scale = gs_ref[...].reshape(1, units)
    up_scale = us_ref[...].reshape(1, units)
    mixed_scale = jnp.concatenate([gate_scale[:, main:], up_scale[:, main:]], axis=1)
    for i in range(2):
        relay[i].wait_recv()
        total += relay_in[i].astype(F32)
    square = jnp.sum(total[:, 2 * units :], axis=1, keepdims=True)
    inv = lax.rsqrt(square / width + 1e-06)
    g = total[:, :main] * inv * gate_scale[:, :main]
    u = total[:, main : 2 * main] * inv * up_scale[:, :main]
    both = total[:, 2 * main : 2 * units] * inv * mixed_scale
    swapped = pltpu.roll(both, rest, 1)
    hid[HOP, :, :main] = (g * jax.nn.sigmoid(g) * u).astype(BF16)
    last = both * jax.nn.sigmoid(both) * swapped
    hid[HOP, :, main:] = jnp.where(tile_lane < rest, last, 0.0).astype(BF16)

    spread = {}
    order = [s * k for k in range(HOP, 0, -1) for s in (1, -1)]
    order += [nz // 2] + [s * k for k in range(nz // 2 - 1, HOP, -1) for s in (1, -1)]
    for d in order:
        e = d % nz
        spread[e] = remote(
            hid.at[HOP],
            hid.at[(HOP - d) % nz],
            hid_sems.at[0, e - 1],
            hid_sems.at[1, e - 1],
            to_z(d),
        )
        spread[e].start()

    groups = 2
    size = nz // groups
    share = size // 2

    def multiply(k):
        for r in range(k * size, (k + 1) * size):
            if r != HOP:
                spread[(HOP - r) % nz].wait_recv()
        rows = hid[k * size : (k + 1) * size].reshape(size * tile, hid.shape[2])
        partial = jnp.dot(rows, down, preferred_element_type=F32)
        pair[k] = partial.reshape(size, tile, feats).astype(BF16)
        copy = remote(
            pair.at[k, pl.ds((1 - core) * share, share)],
            pair_in.at[k],
            pair_sems.at[0, k],
            pair_sems.at[1, k],
            mate,
        )
        copy.start()
        return copy

    def broadcast(k, copy):
        copy.wait_recv()
        own = pair[k, pl.ds(core * share, share)].astype(F32) + pair_in[k].astype(F32)
        chips[k, chip] = own.astype(BF16)
        copies = []
        for d in sorted(range(1, nx), key=lambda d: -min(d, nx - d)):
            to = remote(
                chips.at[k, chip],
                chips.at[k, chip],
                chip_sems.at[0, k, d - 1],
                chip_sems.at[1, k, d - 1],
                to_chip(d),
            )
            to.start()
            copies.append(to)
        return copies

    def finish(k):
        for d in range(1, nx):
            came = chips.at[k, lax.rem(chip + nx - d, nx)]
            remote(came, came, chip_sems.at[0, k, d - 1], chip_sems.at[1, k, d - 1], to_chip(d)).wait_recv()
        branch = chips[k, 0].astype(F32)
        for j in range(1, nx):
            branch += chips[k, j].astype(F32)
        first = k * size + core * share
        for j in range(share):
            own = tok_ref[block(first + j - HOP)].astype(F32)
            mix[first + j] = 0.5 * own + branch[j] * ds_ref[...]
        rows = pl.ds(first, share)
        copy = remote(mix.at[rows], mix.at[rows], mix_sems.at[0, k], mix_sems.at[1, k], mate)
        copy.start()
        other = pl.ds(k * size + (1 - core) * share, share)
        return copy, remote(mix.at[other], mix.at[other], mix_sems.at[0, k], mix_sems.at[1, k], mate)

    swaps = [multiply(0)]
    sends = broadcast(0, swaps[0])
    swaps.append(multiply(1))
    sends += broadcast(1, swaps[1])
    mixes = [finish(0), finish(1)]
    for _, came in mixes:
        came.wait_recv()

    mixed = mix[...].reshape(tokens, feats)
    column = jnp.sum(mixed * mixed, axis=1, keepdims=True)
    place = lax.broadcasted_iota(jnp.int32, (tokens, tokens), 0) + tile * (z + nz - HOP)
    diagonal = lax.rem(place, tokens) == lax.broadcasted_iota(jnp.int32, (tokens, tokens), 1)
    squares[z] = jnp.sum(jnp.where(diagonal, column, 0.0), axis=0, keepdims=True)
    sq_sends = []
    order = sorted(range(1, nz), key=lambda d: -min(d, nz - d))
    for d in order:
        copy = remote(
            squares.at[z], squares.at[z], sq_sems.at[0, d - 1], sq_sems.at[1, d - 1], to_z(d)
        )
        copy.start()
        sq_sends.append(copy)
    out_gain = og_ref[...]
    scaled_mixed = mixed * out_gain
    for d in reversed(order):
        came = squares.at[block(-d)]
        remote(came, came, sq_sems.at[0, d - 1], sq_sems.at[1, d - 1], to_z(d)).wait_recv()
    everything = squares[0]
    for j in range(1, nz):
        everything += squares[j]
    inv_row = lax.rsqrt(everything / width + 1e-06)
    inv_second = jnp.sum(jnp.where(diagonal, inv_row, 0.0), axis=1, keepdims=True)
    result = (scaled_mixed * inv_second).reshape(nz, tile, feats).astype(BF16)
    for r in range(nz):
        out_ref[block(r - HOP)] = result[r]

    for copy in list(far.values()) + list(near.values()) + relay + list(spread.values()):
        copy.wait_send()
    for copy in swaps + sends + [own for own, _ in mixes] + sq_sends:
        copy.wait_send()


def solution(mesh):
    nz, nc = mesh.shape["ra"], mesh.shape["cb"]
    nx = nc // 2

    def on_device(tokens, norm_gain, gw, gs, uw, us, dw, ds, og):
        count, feats = tokens.shape
        units = gw.shape[1]
        padded = -(-units // LANES) * LANES
        tile = count // nz
        cols = 2 * units + LANES
        share = nz // 4
        vmem = pl.BlockSpec(memory_space=pltpu.VMEM)
        hbm = pl.BlockSpec(memory_space=pl.ANY)
        dma = pltpu.SemaphoreType.DMA
        row = lambda v: v.reshape(1, -1)
        out = pl.pallas_call(
            functools.partial(kernel, nz, nc),
            out_shape=jax.ShapeDtypeStruct((nz, tile, feats), BF16),
            in_specs=[vmem, vmem, hbm, vmem, hbm, vmem, hbm, vmem, vmem],
            out_specs=vmem,
            scratch_shapes=[
                pltpu.VMEM((2 * units, feats), F32),
                pltpu.VMEM((padded, feats), F32),
                pltpu.VMEM((nz, tile, cols), BF16),
                pltpu.VMEM((2, HOP - 1, tile, cols), BF16),
                pltpu.VMEM((2, tile, cols // 2), BF16),
                pltpu.VMEM((2, HOP - 1, tile, cols), BF16),
                pltpu.VMEM((2, tile, cols), BF16),
                pltpu.VMEM((2, tile, cols), BF16),
                pltpu.VMEM((nz, tile, padded), BF16),
                pltpu.VMEM((2, nz // 2, tile, feats), BF16),
                pltpu.VMEM((2, share, tile, feats), BF16),
                pltpu.VMEM((2, nx, share, tile, feats), BF16),
                pltpu.VMEM((nz, tile, feats), F32),
                pltpu.VMEM((nz, 1, LANES), F32),
                dma((5,)),
                dma((2, 2, HOP)),
                dma((2, 2, HOP - 1)),
                dma((2, 2)),
                dma((2, nz - 1)),
                dma((2, 2)),
                dma((2, 2, nx - 1)),
                dma((2, 2)),
                dma((2, nz - 1)),
            ],
            compiler_params=pltpu.CompilerParams(collective_id=0, has_side_effects=True),
        )(
            tokens.reshape(nz, tile, feats),
            row(norm_gain),
            gw.T,
            gs,
            uw.T,
            us,
            dw,
            row(ds),
            row(og),
        )
        return out.reshape(count, feats)

    return jax.shard_map(
        on_device,
        mesh=mesh,
        in_specs=(
            P("grp", "ra"),
            P("ra"),
            P("ra", "cb"),
            P("cb"),
            P("ra", "cb"),
            P("cb"),
            P("cb", "ra"),
            P("ra"),
            P("ra"),
        ),
        out_specs=P("grp", "ra"),
        check_vma=False,
    )
```

time: 163 us -> 90 us (0.55)
  blocking collectives: 135 us -> 0 us
  Pallas kernels: 0 us -> 88.3 us
  waiting for transfers between devices: 16.3 us -> 0 us
  starting transfers between devices: 4.12 us -> 0 us
  other arithmetic: 2.23 us -> 0 us
  matrix products: 2.07 us -> 0 us
    all_to_all x4 -> x0, blocking collectives: 135 us -> none  [copy_for_each(): lax.all_to_all(jnp.broadcast_to(value[None], (size, *value.shape)), axis,...]
    pallas_call x0 -> x1, Pallas kernels: none -> 88.3 us  [on_device(): pl.pallas_call(functools.partial(kernel, nz, nc), out_shape=jax.ShapeDtyp...]
    all_to_all x1 -> x0, waiting for transfers between devices: 16.3 us -> none  [summed_on_arrival(): tiles = lax.all_to_all(in_blocks(value, dim, size), axis, 0, 0, tiled=True)]
    all_to_all x1 -> x0, starting transfers between devices: 4.12 us -> none  [summed_on_arrival(): tiles = lax.all_to_all(in_blocks(value, dim, size), axis, 0, 0, tiled=True)]
    dot_general x3 -> x0, matrix products: 2.07 us -> none  [the longest x1 1.48 us: on_device(): up_part = jnp.dot(normed_in, up_local, preferred_element_type=jnp.float32)]
  transfers between devices with their start and end apart: 1 -> 0, of which waited for: 1 -> 0; matrix products, arithmetic and copies ran while one was open for 1% -> 0% of each run, Pallas kernels for 0% -> 0%
where the time goes in v2:
time: 90 us; the launch traced here: 89.8 us
  Pallas kernels  88.3 us (98%)
  local copies, waits for them, and re-layouts  1.47 us (2%)
    pallas_call x1, Pallas kernels, on_device(): pl.pallas_call(functools.partial(kernel, nz, nc), out_shape=jax.ShapeDtyp...  88.3 us

profile of v2, /device:TPU:65, one launch (start us, length us, event | category | flops | bytes accessed | tf_op | source)
XLA Modules:
  0.0 89.8 jit_solution(4077858803028307063)
XLA Ops:
  0.0 88.3 %shard_map.91 = bf16[16,8,256]{2,1,0:T(8,128)(2,1)} custom-call(bf16[16,8,256]{2,1,0:T(8,128)(2,1)} %bitcast.10, f32[1,256]{1,0:T(1,128)} %bitcast.11, f32[704,256]{1,0:T(8,128)} %bitcast.7, f32[704]{0:T(1024)} %gs_ref.1, f32[704,256]{1,0:T(8,128)} %bitcast.8, f32[704]{0:T(1024)} %us_ref.1, f32[704,256]{1,0:T(8,128)} %dw_ref.1, f32[1,256]{1,0:T(1,128)} %bitcast.12, ...), custom_call_target="tpu_custom_call" | custom-call | tf_op jit(solution)/shard_map/pallas_call | solution.py:325
  88.3 1.5 %copy.11 = bf16[128,256]{1,0:T(8,128)(2,1)} copy(bf16[128,256]{1,0:T(8,128)(2,1)} %bitcast.9) | data formatting | bytes 131072

commit v3 on v2

--- a/solution.py
+++ b/solution.py
@@ -33,16 +33,22 @@
 def kernel(
     nz,
     nc,
+    tok_hbm,
+    gain_hbm,
+    gw_ref,
+    gs_hbm,
+    uw_ref,
+    us_hbm,
+    dw_ref,
+    ds_hbm,
+    og_hbm,
+    out_ref,
     tok_ref,
     gain_ref,
-    gw_ref,
     gs_ref,
-    uw_ref,
     us_ref,
-    dw_ref,
     ds_ref,
     og_ref,
-    out_ref,
     gu_v,
     dw_v,
     part,
@@ -102,23 +108,31 @@
         pltpu.make_async_copy(src, dst, load_sem.at[k])
         for k, (src, dst) in enumerate(
             [
+                (tok_hbm, tok_ref),
+                (gain_hbm, gain_ref),
                 (gw_ref.at[:main], gu_v.at[:main]),
                 (uw_ref.at[:main], gu_v.at[main : 2 * main]),
                 (gw_ref.at[main:], gu_v.at[2 * main : 2 * main + rest]),
                 (uw_ref.at[main:], gu_v.at[2 * main + rest :]),
+                (gs_hbm, gs_ref),
+                (us_hbm, us_ref),
                 (dw_ref, dw_v.at[:units]),
+                (ds_hbm, ds_ref),
+                (og_hbm, og_ref),
             ]
         )
     ]
     for copy in loads:
         copy.start()
 
+    for copy in loads[:2]:
+        copy.wait()
     values = tok_ref[...].astype(F32).reshape(tokens, feats)
     scaled = (values * gain_ref[...]).astype(BF16)
     lane = lax.broadcasted_iota(jnp.int32, (tokens, LANES), 1)
     tail = split_tail(jnp.sum(values * values, axis=1, keepdims=True), lane)
     part[:, :, 2 * units :] = tail.reshape(nz, tile, LANES).astype(BF16)
-    for copy in loads[:-1]:
+    for copy in loads[2:6]:
         copy.wait()
     both = lax.dot_general(
         scaled, gu_v[...].astype(BF16), (((1,), (1,)), ((), ())), preferred_element_type=F32
@@ -149,7 +163,8 @@
             )
             near[i, k].start()
 
-    loads[-1].wait()
+    for copy in loads[6:]:
+        copy.wait()
     row = lax.broadcasted_iota(jnp.int32, dw_v.shape, 0)
     down = jnp.where(row < units, dw_v[...], 0.0).astype(BF16)
 
@@ -198,8 +213,7 @@
     hid[HOP, :, main:] = jnp.where(tile_lane < rest, last, 0.0).astype(BF16)
 
     spread = {}
-    order = [s * k for k in range(HOP, 0, -1) for s in (1, -1)]
-    order += [nz // 2] + [s * k for k in range(nz // 2 - 1, HOP, -1) for s in (1, -1)]
+    order = [nz // 2] + [s * k for k in range(nz // 2 - 1, 0, -1) for s in (1, -1)]
     for d in order:
         e = d % nz
         spread[e] = remote(
@@ -261,49 +275,57 @@
             own = tok_ref[block(first + j - HOP)].astype(F32)
             mix[first + j] = 0.5 * own + branch[j] * ds_ref[...]
         rows = pl.ds(first, share)
+        mine = mix[rows].reshape(share * tile, feats)
+        column = jnp.sum(mine * mine, axis=1, keepdims=True)
+        square = jnp.sum(jnp.where(diagonal(first, share), column, 0.0), axis=0, keepdims=True)
         copy = remote(mix.at[rows], mix.at[rows], mix_sems.at[0, k], mix_sems.at[1, k], mate)
         copy.start()
         other = pl.ds(k * size + (1 - core) * share, share)
-        return copy, remote(mix.at[other], mix.at[other], mix_sems.at[0, k], mix_sems.at[1, k], mate)
+        return square, copy, remote(mix.at[other], mix.at[other], mix_sems.at[0, k], mix_sems.at[1, k], mate)
+
+    def diagonal(first, count):
+        place = lax.broadcasted_iota(jnp.int32, (count * tile, tokens), 0)
+        place = lax.rem(place + tile * (z + first + nz - HOP), tokens)
+        return place == lax.broadcasted_iota(jnp.int32, (count * tile, tokens), 1)
 
     swaps = [multiply(0)]
     sends = broadcast(0, swaps[0])
     swaps.append(multiply(1))
     sends += broadcast(1, swaps[1])
-    mixes = [finish(0), finish(1)]
-    for _, came in mixes:
-        came.wait_recv()
-
-    mixed = mix[...].reshape(tokens, feats)
-    column = jnp.sum(mixed * mixed, axis=1, keepdims=True)
-    place = lax.broadcasted_iota(jnp.int32, (tokens, tokens), 0) + tile * (z + nz - HOP)
-    diagonal = lax.rem(place, tokens) == lax.broadcasted_iota(jnp.int32, (tokens, tokens), 1)
-    squares[z] = jnp.sum(jnp.where(diagonal, column, 0.0), axis=0, keepdims=True)
-    sq_sends = []
+    near_squares, near_mix, near_came = finish(0)
+    far_squares, far_mix, far_came = finish(1)
+
+    squares[core, z] = near_squares + far_squares
+    own = squares.at[core, z]
+    sq_sends = [remote(own, own, sq_sems.at[0, 0, 0], sq_sems.at[1, 0, 0], mate)]
     order = sorted(range(1, nz), key=lambda d: -min(d, nz - d))
     for d in order:
-        copy = remote(
-            squares.at[z], squares.at[z], sq_sems.at[0, d - 1], sq_sems.at[1, d - 1], to_z(d)
-        )
+        for t in range(2):
+            peer = {"ra": lax.rem(z + d, nz), "cb": chip * 2 + lax.rem(core + t, 2)}
+            sq_sends.append(remote(own, own, sq_sems.at[0, t, d], sq_sems.at[1, t, d], peer))
+    for copy in sq_sends:
         copy.start()
-        sq_sends.append(copy)
-    out_gain = og_ref[...]
-    scaled_mixed = mixed * out_gain
+    near_came.wait_recv()
+    far_came.wait_recv()
+    scaled_mixed = mix[...].reshape(tokens, feats) * og_ref[...]
+    came = squares.at[1 - core, z]
+    remote(came, came, sq_sems.at[0, 0, 0], sq_sems.at[1, 0, 0], mate).wait_recv()
     for d in reversed(order):
-        came = squares.at[block(-d)]
-        remote(came, came, sq_sems.at[0, d - 1], sq_sems.at[1, d - 1], to_z(d)).wait_recv()
-    everything = squares[0]
-    for j in range(1, nz):
-        everything += squares[j]
+        for t in range(2):
+            came = squares.at[lax.rem(core + t, 2), block(-d)]
+            remote(came, came, sq_sems.at[0, t, d], sq_sems.at[1, t, d], mate).wait_recv()
+    everything = squares[0, 0]
+    for j in range(1, 2 * nz):
+        everything += squares[j // nz, j % nz]
     inv_row = lax.rsqrt(everything / width + 1e-06)
-    inv_second = jnp.sum(jnp.where(diagonal, inv_row, 0.0), axis=1, keepdims=True)
+    inv_second = jnp.sum(jnp.where(diagonal(0, nz), inv_row, 0.0), axis=1, keepdims=True)
     result = (scaled_mixed * inv_second).reshape(nz, tile, feats).astype(BF16)
     for r in range(nz):
         out_ref[block(r - HOP)] = result[r]
 
     for copy in list(far.values()) + list(near.values()) + relay + list(spread.values()):
         copy.wait_send()
-    for copy in swaps + sends + [own for own, _ in mixes] + sq_sends:
+    for copy in swaps + sends + [near_mix, far_mix] + sq_sends:
         copy.wait_send()
 
 
@@ -319,15 +341,21 @@
         cols = 2 * units + LANES
         share = nz // 4
         vmem = pl.BlockSpec(memory_space=pltpu.VMEM)
-        hbm = pl.BlockSpec(memory_space=pl.ANY)
+        hbm = pl.BlockSpec(memory_space=pltpu.HBM)
         dma = pltpu.SemaphoreType.DMA
         row = lambda v: v.reshape(1, -1)
         out = pl.pallas_call(
             functools.partial(kernel, nz, nc),
-            out_shape=jax.ShapeDtypeStruct((nz, tile, feats), BF16),
-            in_specs=[vmem, vmem, hbm, vmem, hbm, vmem, hbm, vmem, vmem],
+            out_shape=pltpu.VMEM((nz, tile, feats), BF16),
+            in_specs=[hbm] * 9,
             out_specs=vmem,
             scratch_shapes=[
+                pltpu.VMEM((nz, tile, feats), BF16),
+                pltpu.VMEM((1, feats), F32),
+                pltpu.VMEM((units,), F32),
+                pltpu.VMEM((units,), F32),
+                pltpu.VMEM((1, feats), F32),
+                pltpu.VMEM((1, feats), F32),
                 pltpu.VMEM((2 * units, feats), F32),
                 pltpu.VMEM((padded, feats), F32),
                 pltpu.VMEM((nz, tile, cols), BF16),
@@ -341,8 +369,8 @@
                 pltpu.VMEM((2, share, tile, feats), BF16),
                 pltpu.VMEM((2, nx, share, tile, feats), BF16),
                 pltpu.VMEM((nz, tile, feats), F32),
-                pltpu.VMEM((nz, 1, LANES), F32),
-                dma((5,)),
+                pltpu.VMEM((2, nz, 1, LANES), F32),
+                dma((11,)),
                 dma((2, 2, HOP)),
                 dma((2, 2, HOP - 1)),
                 dma((2, 2)),
@@ -350,9 +378,11 @@
                 dma((2, 2)),
                 dma((2, 2, nx - 1)),
                 dma((2, 2)),
-                dma((2, nz - 1)),
+                dma((2, 2, nz)),
             ],
-            compiler_params=pltpu.CompilerParams(collective_id=0, has_side_effects=True),
+            compiler_params=pltpu.CompilerParams(
+                collective_id=0, has_side_effects=True
+            ),
         )(
             tokens.reshape(nz, tile, feats),
             row(norm_gain),

time: 90 us -> 89.1 us (0.990)
  no operation moved by 1% of the time
where the time goes in v3:
time: 89.1 us; the launch traced here: 89 us
  Pallas kernels  88.3 us (99%)
    pallas_call x1, Pallas kernels, on_device(): pl.pallas_call(functools.partial(kernel, nz, nc), out_shape=pltpu.VMEM((n...  88.3 us

profile of v3, /device:TPU:65, one launch (start us, length us, event | category | flops | bytes accessed | tf_op | source)
XLA Modules:
  0.0 89.0 jit_solution(5136771162366339795)
XLA Ops:
  0.0 88.3 %shard_map.91 = bf16[16,8,256]{2,1,0:T(8,128)(2,1)S(1)} custom-call(bf16[16,8,256]{2,1,0:T(8,128)(2,1)} %bitcast.10, f32[1,256]{1,0:T(1,128)} %bitcast.11, f32[704,256]{1,0:T(8,128)} %bitcast.8, f32[704]{0:T(1024)} %gs_hbm.1, f32[704,256]{1,0:T(8,128)} %bitcast.9, f32[704]{0:T(1024)} %us_hbm.1, f32[704,256]{1,0:T(8,128)} %dw_ref.1, f32[1,256]{1,0:T(1,128)} %bitcast.12, ...), custom_call_target="tpu_custom_call" | custom-call | tf_op jit(solution)/shard_map/pallas_call | solution.py:347
  88.3 0.6 copy.11

commit v4 on v3

--- a/solution.py
+++ b/solution.py
@@ -64,6 +64,7 @@
     mix,
     squares,
     load_sem,
+    ready,
     far_sems,
     near_sems,
     relay_sems,
@@ -98,10 +99,22 @@
     def block(d):
         return lax.rem(z + d + 2 * nz, nz)
 
+    near_peers = [(i, k) for k in range(HOP, 0, -1) for i in (0, 1)]
+    rising = [(0, k) for k in range(1, HOP + 1)] + [(1, k) for k in range(HOP, 0, -1)]
+    sign = (1, -1)
+
+    def lower(i, k):
+        return block(sign[i] * k) < z
+
     barrier = pltpu.get_barrier_semaphore()
-    peers = [to_z(s * d) for d in range(1, HOP + 1) for s in (1, -1)]
-    peers += [to_chip(d) for d in range(1, nx)] + [mate]
-    for peer in peers:
+    x_peers = [to_chip(d) for d in range(1, nx)] + [mate]
+    for i, k in near_peers:
+
+        @pl.when(jnp.logical_not(lower(i, k)))
+        def _():
+            pl.semaphore_signal(barrier, inc=1, device_id=to_z(sign[i] * k), device_id_type=MESH)
+
+    for peer in x_peers:
         pl.semaphore_signal(barrier, inc=1, device_id=peer, device_id_type=MESH)
 
     loads = [
@@ -125,6 +138,16 @@
     for copy in loads:
         copy.start()
 
+    count = len(x_peers) + sum(jnp.where(lower(i, k), 1, 0) for i, k in near_peers)
+    pl.semaphore_wait(barrier, count)
+    for i, k in near_peers:
+
+        @pl.when(lower(i, k))
+        def _():
+            pl.semaphore_signal(
+                ready.at[1 - i, k - 1], inc=1, device_id=to_z(sign[i] * k), device_id_type=MESH
+            )
+
     for copy in loads[:2]:
         copy.wait()
     values = tok_ref[...].astype(F32).reshape(tokens, feats)
@@ -139,29 +162,37 @@
     )
     part[:, :, : 2 * units] = both.reshape(nz, tile, 2 * units).astype(BF16)
 
-    pl.semaphore_wait(barrier, len(peers))
-
-    waiting = []
     far = {}
-    for k in range(HOP, 0, -1):
-        for i, s in enumerate((1, -1)):
-            src = part.at[block(s * (k + HOP))]
-            dst = far_in.at[i, k - 1] if k < HOP else far_in_half.at[i]
-            if k == HOP:
-                src = part.at[block(s * (k + HOP)), :, halves[i]]
-            far[i, k] = remote(src, dst, far_sems.at[0, i, k - 1], far_sems.at[1, i, k - 1], to_z(s * k))
+    near = {}
+    for i, k in near_peers:
+        src = part.at[block(sign[i] * (k + HOP))]
+        dst = far_in.at[i, k - 1] if k < HOP else far_in_half.at[i]
+        if k == HOP:
+            src = part.at[block(sign[i] * (k + HOP)), :, halves[i]]
+        sems = far_sems.at[0, i, k - 1], far_sems.at[1, i, k - 1]
+        far[i, k] = remote(src, dst, *sems, to_z(sign[i] * k))
+        if k < HOP:
+            sems = near_sems.at[0, i, k - 1], near_sems.at[1, i, k - 1]
+            near[i, k] = remote(
+                part.at[block(sign[i] * k)], near_in.at[i, k - 1], *sems, to_z(sign[i] * k)
+            )
+
+    for table in (far, near):
+        for i, k in near_peers:
+            if (i, k) in table:
+
+                @pl.when(lower(i, k))
+                def _():
+                    table[i, k].start()
+
+    for i, k in rising:
+
+        @pl.when(jnp.logical_not(lower(i, k)))
+        def _():
+            pl.semaphore_wait(ready.at[i, k - 1], 1)
             far[i, k].start()
-    near = {}
-    for k in range(HOP - 1, 0, -1):
-        for i, s in enumerate((1, -1)):
-            near[i, k] = remote(
-                part.at[block(s * k)],
-                near_in.at[i, k - 1],
-                near_sems.at[0, i, k - 1],
-                near_sems.at[1, i, k - 1],
-                to_z(s * k),
-            )
-            near[i, k].start()
+            if k < HOP:
+                near[i, k].start()
 
     for copy in loads[6:]:
         copy.wait()
@@ -169,27 +200,38 @@
     down = jnp.where(row < units, dw_v[...], 0.0).astype(BF16)
 
     tile_lane = lax.broadcasted_iota(jnp.int32, (tile, LANES), 1)
-    relay = []
-    for i, s in enumerate((1, -1)):
+    relay = [
+        remote(
+            relay_out.at[i], relay_in.at[i], relay_sems.at[0, i], relay_sems.at[1, i], to_z(sign[i] * HOP)
+        )
+        for i in (0, 1)
+    ]
+
+    def pass_on(i):
         for k in range(1, HOP + 1):
             far[i, k].wait_recv()
-        total = part[block(s * HOP)].astype(F32)
+        total = part[block(sign[i] * HOP)].astype(F32)
         for k in range(1, HOP):
             total += far_in[i, k - 1].astype(F32)
-        half = far_in_half[i].astype(F32)
         pieces = [total[:, halves[0]], total[:, halves[1]]]
-        pieces[i] += half
+        pieces[i] += far_in_half[i].astype(F32)
         last = pieces[1][:, -LANES:]
         relay_out[i, :, halves[0]] = pieces[0].astype(BF16)
         relay_out[i, :, cols // 2 : cols - LANES] = pieces[1][:, :-LANES].astype(BF16)
         relay_out[i, :, cols - LANES :] = split_tail(
             jnp.sum(last, axis=1, keepdims=True), tile_lane
         ).astype(BF16)
-        copy = remote(
-            relay_out.at[i], relay_in.at[i], relay_sems.at[0, i], relay_sems.at[1, i], to_z(s * HOP)
-        )
-        copy.start()
-        relay.append(copy)
+        relay[i].start()
+
+    @pl.when(z >= HOP)
+    def _():
+        pass_on(0)
+
+    pass_on(1)
+
+    @pl.when(z < HOP)
+    def _():
+        pass_on(0)
 
     total = part[z].astype(F32)
     for k in range(1, HOP):
@@ -212,27 +254,42 @@
     last = both * jax.nn.sigmoid(both) * swapped
     hid[HOP, :, main:] = jnp.where(tile_lane < rest, last, 0.0).astype(BF16)
 
+    hid_cols = hid.shape[2]
+    hid_halves = (slice(0, hid_cols // 2), slice(hid_cols // 2, hid_cols))
     spread = {}
-    order = [nz // 2] + [s * k for k in range(nz // 2 - 1, 0, -1) for s in (1, -1)]
-    for d in order:
-        e = d % nz
-        spread[e] = remote(
+    for i, k in near_peers:
+        spread[i, k] = remote(
             hid.at[HOP],
-            hid.at[(HOP - d) % nz],
-            hid_sems.at[0, e - 1],
-            hid_sems.at[1, e - 1],
-            to_z(d),
+            hid.at[(HOP - sign[i] * k) % nz],
+            hid_sems.at[0, 0, i, k - 1],
+            hid_sems.at[1, 0, i, k - 1],
+            to_z(sign[i] * k),
         )
-        spread[e].start()
+        spread[i, k].start()
+    onward = {}
+    for i in (0, 1):
+        spread[i, HOP].wait_recv()
+        for k in range(HOP, 0, -1):
+            src = hid.at[(HOP - sign[i] * HOP) % nz]
+            dst = hid.at[(HOP - sign[i] * (HOP + k)) % nz]
+            if k == HOP:
+                src = hid.at[(HOP - sign[i] * HOP) % nz, :, hid_halves[i]]
+                dst = hid.at[(HOP - sign[i] * (HOP + k)) % nz, :, hid_halves[i]]
+            onward[i, k] = remote(
+                src, dst, hid_sems.at[0, 1, i, k - 1], hid_sems.at[1, 1, i, k - 1], to_z(sign[i] * k)
+            )
+            onward[i, k].start()
 
     groups = 2
     size = nz // groups
     share = size // 2
 
     def multiply(k):
-        for r in range(k * size, (k + 1) * size):
-            if r != HOP:
-                spread[(HOP - r) % nz].wait_recv()
+        for i, j in near_peers:
+            if k == 1:
+                onward[i, j].wait_recv()
+            elif j < HOP:
+                spread[i, j].wait_recv()
         rows = hid[k * size : (k + 1) * size].reshape(size * tile, hid.shape[2])
         partial = jnp.dot(rows, down, preferred_element_type=F32)
         pair[k] = partial.reshape(size, tile, feats).astype(BF16)
@@ -323,7 +380,8 @@
     for r in range(nz):
         out_ref[block(r - HOP)] = result[r]
 
-    for copy in list(far.values()) + list(near.values()) + relay + list(spread.values()):
+    tables = (far, near, spread, onward)
+    for copy in relay + [copy for table in tables for copy in table.values()]:
         copy.wait_send()
     for copy in swaps + sends + [near_mix, far_mix] + sq_sends:
         copy.wait_send()
@@ -371,10 +429,11 @@
                 pltpu.VMEM((nz, tile, feats), F32),
                 pltpu.VMEM((2, nz, 1, LANES), F32),
                 dma((11,)),
+                pltpu.SemaphoreType.REGULAR((2, HOP)),
                 dma((2, 2, HOP)),
                 dma((2, 2, HOP - 1)),
                 dma((2, 2)),
-                dma((2, nz - 1)),
+                dma((2, 2, 2, HOP)),
                 dma((2, 2)),
                 dma((2, 2, nx - 1)),
                 dma((2, 2)),

time: 89.1 us -> 86.7 us (0.973)
  Pallas kernels: 88.3 us -> 85.9 us
    pallas_call x1, Pallas kernels: 88.3 us -> 85.9 us  [on_device(): pl.pallas_call(functools.partial(kernel, nz, nc), out_shape=pltpu.VMEM((n...]
where the time goes in v4:
time: 86.7 us; the launch traced here: 86.6 us
  Pallas kernels  85.9 us (99%)
    pallas_call x1, Pallas kernels, on_device(): pl.pallas_call(functools.partial(kernel, nz, nc), out_shape=pltpu.VMEM((n...  85.9 us

profile of v4, /device:TPU:65, one launch (start us, length us, event | category | flops | bytes accessed | tf_op | source)
XLA Modules:
  0.0 86.6 jit_solution(18093212838036621300)
XLA Ops:
  0.0 85.9 %shard_map.91 = bf16[16,8,256]{2,1,0:T(8,128)(2,1)S(1)} custom-call(bf16[16,8,256]{2,1,0:T(8,128)(2,1)} %bitcast.10, f32[1,256]{1,0:T(1,128)} %bitcast.11, f32[704,256]{1,0:T(8,128)} %bitcast.8, f32[704]{0:T(1024)} %gs_hbm.1, f32[704,256]{1,0:T(8,128)} %bitcast.9, f32[704]{0:T(1024)} %us_hbm.1, f32[704,256]{1,0:T(8,128)} %dw_ref.1, f32[1,256]{1,0:T(1,128)} %bitcast.12, ...), custom_call_target="tpu_custom_call" | custom-call | tf_op jit(solution)/shard_map/pallas_call | solution.py:405
  86.0 0.6 copy.11

commit v5 on v4

--- a/solution.py
+++ b/solution.py
@@ -23,6 +23,14 @@
         device_id=peer,
         device_id_type=MESH,
     )
+
+
+def arrived(ref, sem, peer):
+    remote(ref, ref, sem, sem, peer).wait_recv()
+
+
+def left(ref, sem, peer):
+    remote(ref, ref, sem, sem, peer).wait_send()
 
 
 def split_tail(column, lane):
@@ -65,14 +73,21 @@
     squares,
     load_sem,
     ready,
-    far_sems,
-    near_sems,
-    relay_sems,
-    hid_sems,
-    pair_sems,
-    chip_sems,
-    mix_sems,
-    sq_sems,
+    x_ready,
+    rs_send,
+    far_recv,
+    near_recv,
+    relay_recv,
+    hid_send,
+    hid_recv,
+    pair_send,
+    pair_recv,
+    chip_send,
+    chip_recv,
+    mix_send,
+    mix_recv,
+    sq_send,
+    sq_recv,
 ):
     z = lax.axis_index("ra")
     cb = lax.axis_index("cb")
@@ -106,16 +121,27 @@
     def lower(i, k):
         return block(sign[i] * k) < z
 
+    def turn(c):
+        return jnp.minimum(c, nx - c) * nx + c
+
+    def x_lower(d):
+        return core == 0 if d == 0 else turn(lax.rem(chip + d, nx)) < turn(chip)
+
+    def to_x(d):
+        return mate if d == 0 else to_chip(d)
+
     barrier = pltpu.get_barrier_semaphore()
-    x_peers = [to_chip(d) for d in range(1, nx)] + [mate]
     for i, k in near_peers:
 
         @pl.when(jnp.logical_not(lower(i, k)))
         def _():
             pl.semaphore_signal(barrier, inc=1, device_id=to_z(sign[i] * k), device_id_type=MESH)
 
-    for peer in x_peers:
-        pl.semaphore_signal(barrier, inc=1, device_id=peer, device_id_type=MESH)
+    for d in range(nx):
+
+        @pl.when(jnp.logical_not(x_lower(d)))
+        def _():
+            pl.semaphore_signal(barrier, inc=1, device_id=to_x(d), device_id_type=MESH)
 
     loads = [
         pltpu.make_async_copy(src, dst, load_sem.at[k])
@@ -138,14 +164,27 @@
     for copy in loads:
         copy.start()
 
-    count = len(x_peers) + sum(jnp.where(lower(i, k), 1, 0) for i, k in near_peers)
-    pl.semaphore_wait(barrier, count)
+    count = sum(jnp.where(lower(i, k), 1, 0) for i, k in near_peers)
+    count += sum(jnp.where(x_lower(d), 1, 0) for d in range(nx))
+
+    @pl.when(count > 0)
+    def _():
+        pl.semaphore_wait(barrier, count)
+
     for i, k in near_peers:
 
         @pl.when(lower(i, k))
         def _():
             pl.semaphore_signal(
                 ready.at[1 - i, k - 1], inc=1, device_id=to_z(sign[i] * k), device_id_type=MESH
+            )
+
+    for d in range(nx):
+
+        @pl.when(x_lower(d))
+        def _():
+            pl.semaphore_signal(
+                x_ready.at[(nx - d) % nx], inc=1, device_id=to_x(d), device_id_type=MESH
             )
 
     for copy in loads[:2]:
@@ -169,12 +208,14 @@
         dst = far_in.at[i, k - 1] if k < HOP else far_in_half.at[i]
         if k == HOP:
             src = part.at[block(sign[i] * (k + HOP)), :, halves[i]]
-        sems = far_sems.at[0, i, k - 1], far_sems.at[1, i, k - 1]
-        far[i, k] = remote(src, dst, *sems, to_z(sign[i] * k))
+        far[i, k] = remote(src, dst, rs_send, far_recv.at[i], to_z(sign[i] * k))
         if k < HOP:
-            sems = near_sems.at[0, i, k - 1], near_sems.at[1, i, k - 1]
             near[i, k] = remote(
-                part.at[block(sign[i] * k)], near_in.at[i, k - 1], *sems, to_z(sign[i] * k)
+                part.at[block(sign[i] * k)],
+                near_in.at[i, k - 1],
+                rs_send,
+                near_recv,
+                to_z(sign[i] * k),
             )
 
     for table in (far, near):
@@ -201,15 +242,12 @@
 
     tile_lane = lax.broadcasted_iota(jnp.int32, (tile, LANES), 1)
     relay = [
-        remote(
-            relay_out.at[i], relay_in.at[i], relay_sems.at[0, i], relay_sems.at[1, i], to_z(sign[i] * HOP)
-        )
+        remote(relay_out.at[i], relay_in.at[i], rs_send, relay_recv, to_z(sign[i] * HOP))
         for i in (0, 1)
     ]
 
     def pass_on(i):
-        for k in range(1, HOP + 1):
-            far[i, k].wait_recv()
+        arrived(part.at[: 2 * HOP - 1, :, halves[0]], far_recv.at[i], mate)
         total = part[block(sign[i] * HOP)].astype(F32)
         for k in range(1, HOP):
             total += far_in[i, k - 1].astype(F32)
@@ -234,15 +272,15 @@
         pass_on(0)
 
     total = part[z].astype(F32)
+    arrived(near_in, near_recv, mate)
     for k in range(1, HOP):
         for i in range(2):
-            near[i, k].wait_recv()
             total += near_in[i, k - 1].astype(F32)
     gate_scale = gs_ref[...].reshape(1, units)
     up_scale = us_ref[...].reshape(1, units)
     mixed_scale = jnp.concatenate([gate_scale[:, main:], up_scale[:, main:]], axis=1)
+    arrived(relay_in, relay_recv, mate)
     for i in range(2):
-        relay[i].wait_recv()
         total += relay_in[i].astype(F32)
     square = jnp.sum(total[:, 2 * units :], axis=1, keepdims=True)
     inv = lax.rsqrt(square / width + 1e-06)
@@ -261,23 +299,21 @@
         spread[i, k] = remote(
             hid.at[HOP],
             hid.at[(HOP - sign[i] * k) % nz],
-            hid_sems.at[0, 0, i, k - 1],
-            hid_sems.at[1, 0, i, k - 1],
+            hid_send,
+            hid_recv.at[i if k == HOP else 2],
             to_z(sign[i] * k),
         )
         spread[i, k].start()
     onward = {}
     for i in (0, 1):
-        spread[i, HOP].wait_recv()
+        arrived(hid.at[0], hid_recv.at[i], mate)
         for k in range(HOP, 0, -1):
             src = hid.at[(HOP - sign[i] * HOP) % nz]
             dst = hid.at[(HOP - sign[i] * (HOP + k)) % nz]
             if k == HOP:
                 src = hid.at[(HOP - sign[i] * HOP) % nz, :, hid_halves[i]]
                 dst = hid.at[(HOP - sign[i] * (HOP + k)) % nz, :, hid_halves[i]]
-            onward[i, k] = remote(
-                src, dst, hid_sems.at[0, 1, i, k - 1], hid_sems.at[1, 1, i, k - 1], to_z(sign[i] * k)
-            )
+            onward[i, k] = remote(src, dst, hid_send, hid_recv.at[3], to_z(sign[i] * k))
             onward[i, k].start()
 
     groups = 2
@@ -285,45 +321,35 @@
     share = size // 2
 
     def multiply(k):
-        for i, j in near_peers:
-            if k == 1:
-                onward[i, j].wait_recv()
-            elif j < HOP:
-                spread[i, j].wait_recv()
+        arrived(hid.at[: 2 * HOP - 2 + k], hid_recv.at[2 + k], mate)
         rows = hid[k * size : (k + 1) * size].reshape(size * tile, hid.shape[2])
         partial = jnp.dot(rows, down, preferred_element_type=F32)
         pair[k] = partial.reshape(size, tile, feats).astype(BF16)
         copy = remote(
             pair.at[k, pl.ds((1 - core) * share, share)],
             pair_in.at[k],
-            pair_sems.at[0, k],
-            pair_sems.at[1, k],
+            pair_send,
+            pair_recv.at[k],
             mate,
         )
         copy.start()
-        return copy
-
-    def broadcast(k, copy):
-        copy.wait_recv()
+
+    def broadcast(k):
+        arrived(pair_in.at[k], pair_recv.at[k], mate)
         own = pair[k, pl.ds(core * share, share)].astype(F32) + pair_in[k].astype(F32)
         chips[k, chip] = own.astype(BF16)
-        copies = []
         for d in sorted(range(1, nx), key=lambda d: -min(d, nx - d)):
             to = remote(
                 chips.at[k, chip],
                 chips.at[k, chip],
-                chip_sems.at[0, k, d - 1],
-                chip_sems.at[1, k, d - 1],
+                chip_send,
+                chip_recv.at[k],
                 to_chip(d),
             )
             to.start()
-            copies.append(to)
-        return copies
 
     def finish(k):
-        for d in range(1, nx):
-            came = chips.at[k, lax.rem(chip + nx - d, nx)]
-            remote(came, came, chip_sems.at[0, k, d - 1], chip_sems.at[1, k, d - 1], to_chip(d)).wait_recv()
+        arrived(chips.at[k, : nx - 1], chip_recv.at[k], mate)
         branch = chips[k, 0].astype(F32)
         for j in range(1, nx):
             branch += chips[k, j].astype(F32)
@@ -335,56 +361,57 @@
         mine = mix[rows].reshape(share * tile, feats)
         column = jnp.sum(mine * mine, axis=1, keepdims=True)
         square = jnp.sum(jnp.where(diagonal(first, share), column, 0.0), axis=0, keepdims=True)
-        copy = remote(mix.at[rows], mix.at[rows], mix_sems.at[0, k], mix_sems.at[1, k], mate)
-        copy.start()
-        other = pl.ds(k * size + (1 - core) * share, share)
-        return square, copy, remote(mix.at[other], mix.at[other], mix_sems.at[0, k], mix_sems.at[1, k], mate)
+        remote(mix.at[rows], mix.at[rows], mix_send, mix_recv, mate).start()
+        return square
 
     def diagonal(first, count):
         place = lax.broadcasted_iota(jnp.int32, (count * tile, tokens), 0)
         place = lax.rem(place + tile * (z + first + nz - HOP), tokens)
         return place == lax.broadcasted_iota(jnp.int32, (count * tile, tokens), 1)
 
-    swaps = [multiply(0)]
-    sends = broadcast(0, swaps[0])
-    swaps.append(multiply(1))
-    sends += broadcast(1, swaps[1])
-    near_squares, near_mix, near_came = finish(0)
-    far_squares, far_mix, far_came = finish(1)
-
-    squares[core, z] = near_squares + far_squares
-    own = squares.at[core, z]
-    sq_sends = [remote(own, own, sq_sems.at[0, 0, 0], sq_sems.at[1, 0, 0], mate)]
+    @pl.when(jnp.logical_not(x_lower(0)))
+    def _():
+        pl.semaphore_wait(x_ready.at[0], 1)
+
+    multiply(0)
+    for d in range(1, nx):
+
+        @pl.when(jnp.logical_not(x_lower(d)))
+        def _():
+            pl.semaphore_wait(x_ready.at[d], 1)
+
+    broadcast(0)
+    multiply(1)
+    broadcast(1)
+    near_squares = finish(0)
+    far_squares = finish(1)
+
+    squares[core * nz + z] = near_squares + far_squares
+    own = squares.at[core * nz + z]
     order = sorted(range(1, nz), key=lambda d: -min(d, nz - d))
     for d in order:
         for t in range(2):
             peer = {"ra": lax.rem(z + d, nz), "cb": chip * 2 + lax.rem(core + t, 2)}
-            sq_sends.append(remote(own, own, sq_sems.at[0, t, d], sq_sems.at[1, t, d], peer))
-    for copy in sq_sends:
-        copy.start()
-    near_came.wait_recv()
-    far_came.wait_recv()
+            remote(own, own, sq_send, sq_recv, peer).start()
+    remote(own, own, sq_send, sq_recv, mate).start()
+    arrived(mix.at[: 2 * share], mix_recv, mate)
     scaled_mixed = mix[...].reshape(tokens, feats) * og_ref[...]
-    came = squares.at[1 - core, z]
-    remote(came, came, sq_sems.at[0, 0, 0], sq_sems.at[1, 0, 0], mate).wait_recv()
-    for d in reversed(order):
-        for t in range(2):
-            came = squares.at[lax.rem(core + t, 2), block(-d)]
-            remote(came, came, sq_sems.at[0, t, d], sq_sems.at[1, t, d], mate).wait_recv()
-    everything = squares[0, 0]
+    arrived(squares.at[: 2 * nz - 1], sq_recv, mate)
+    everything = squares[0]
     for j in range(1, 2 * nz):
-        everything += squares[j // nz, j % nz]
+        everything += squares[j]
     inv_row = lax.rsqrt(everything / width + 1e-06)
     inv_second = jnp.sum(jnp.where(diagonal(0, nz), inv_row, 0.0), axis=1, keepdims=True)
     result = (scaled_mixed * inv_second).reshape(nz, tile, feats).astype(BF16)
     for r in range(nz):
         out_ref[block(r - HOP)] = result[r]
 
-    tables = (far, near, spread, onward)
-    for copy in relay + [copy for table in tables for copy in table.values()]:
-        copy.wait_send()
-    for copy in swaps + sends + [near_mix, far_mix] + sq_sends:
-        copy.wait_send()
+    left(part.at[: 4 * HOP - 1], rs_send, mate)
+    left(hid.at[: 4 * HOP - 1], hid_send, mate)
+    left(pair.at[0], pair_send, mate)
+    left(chips.at[:, : nx - 1], chip_send, mate)
+    left(mix.at[: 2 * share], mix_send, mate)
+    left(squares.at[: 2 * nz - 1], sq_send, mate)
 
 
 def solution(mesh):
@@ -427,17 +454,24 @@
                 pltpu.VMEM((2, share, tile, feats), BF16),
                 pltpu.VMEM((2, nx, share, tile, feats), BF16),
                 pltpu.VMEM((nz, tile, feats), F32),
-                pltpu.VMEM((2, nz, 1, LANES), F32),
+                pltpu.VMEM((2 * nz, 1, LANES), F32),
                 dma((11,)),
                 pltpu.SemaphoreType.REGULAR((2, HOP)),
-                dma((2, 2, HOP)),
-                dma((2, 2, HOP - 1)),
-                dma((2, 2)),
-                dma((2, 2, 2, HOP)),
-                dma((2, 2)),
-                dma((2, 2, nx - 1)),
-                dma((2, 2)),
-                dma((2, 2, nz)),
+                pltpu.SemaphoreType.REGULAR((nx,)),
+                dma,
+                dma((2,)),
+                dma,
+                dma,
+                dma,
+                dma((4,)),
+                dma,
+                dma((2,)),
+                dma,
+                dma((2,)),
+                dma,
+                dma,
+                dma,
+                dma,
             ],
             compiler_params=pltpu.CompilerParams(
                 collective_id=0, has_side_effects=True

time: 86.7 us -> 84.9 us (0.979)
  Pallas kernels: 85.9 us -> 84.1 us
    pallas_call x1, Pallas kernels: 85.9 us -> 84.1 us  [on_device(): pl.pallas_call(functools.partial(kernel, nz, nc), out_shape=pltpu.VMEM((n...]
where the time goes in v5:
time: 84.9 us; the launch traced here: 84.8 us
  Pallas kernels  84.1 us (99%)
    pallas_call x1, Pallas kernels, on_device(): pl.pallas_call(functools.partial(kernel, nz, nc), out_shape=pltpu.VMEM((n...  84.1 us

profile of v5, /device:TPU:65, one launch (start us, length us, event | category | flops | bytes accessed | tf_op | source)
XLA Modules:
  0.0 84.8 jit_solution(6566002191219034492)
XLA Ops:
  0.0 84.1 %shard_map.91 = bf16[16,8,256]{2,1,0:T(8,128)(2,1)S(1)} custom-call(bf16[16,8,256]{2,1,0:T(8,128)(2,1)} %bitcast.10, f32[1,256]{1,0:T(1,128)} %bitcast.11, f32[704,256]{1,0:T(8,128)} %bitcast.8, f32[704]{0:T(1024)} %gs_hbm.1, f32[704,256]{1,0:T(8,128)} %bitcast.9, f32[704]{0:T(1024)} %us_hbm.1, f32[704,256]{1,0:T(8,128)} %dw_ref.1, f32[1,256]{1,0:T(1,128)} %bitcast.12, ...), custom_call_target="tpu_custom_call" | custom-call | tf_op jit(solution)/shard_map/pallas_call | solution.py:432
  84.1 0.6 copy.11

commit v6 on v5

--- a/solution.py
+++ b/solution.py
@@ -74,6 +74,7 @@
     load_sem,
     ready,
     x_ready,
+    word,
     rs_send,
     far_recv,
     near_recv,
@@ -130,6 +131,7 @@
     def to_x(d):
         return mate if d == 0 else to_chip(d)
 
+    beside = (0, 1, nx - 1)
     barrier = pltpu.get_barrier_semaphore()
     for i, k in near_peers:
 
@@ -137,7 +139,7 @@
         def _():
             pl.semaphore_signal(barrier, inc=1, device_id=to_z(sign[i] * k), device_id_type=MESH)
 
-    for d in range(nx):
+    for d in beside:
 
         @pl.when(jnp.logical_not(x_lower(d)))
         def _():
@@ -165,7 +167,7 @@
         copy.start()
 
     count = sum(jnp.where(lower(i, k), 1, 0) for i, k in near_peers)
-    count += sum(jnp.where(x_lower(d), 1, 0) for d in range(nx))
+    count += sum(jnp.where(x_lower(d), 1, 0) for d in beside)
 
     @pl.when(count > 0)
     def _():
@@ -179,12 +181,12 @@
                 ready.at[1 - i, k - 1], inc=1, device_id=to_z(sign[i] * k), device_id_type=MESH
             )
 
-    for d in range(nx):
+    for n, d in enumerate(beside):
 
         @pl.when(x_lower(d))
         def _():
             pl.semaphore_signal(
-                x_ready.at[(nx - d) % nx], inc=1, device_id=to_x(d), device_id_type=MESH
+                x_ready.at[(3 - n) % 3], inc=1, device_id=to_x(d), device_id_type=MESH
             )
 
     for copy in loads[:2]:
@@ -235,6 +237,22 @@
             if k < HOP:
                 near[i, k].start()
 
+    def tell(m):
+        for n, d in ((0, 1), (1, nx - 1)):
+            pl.semaphore_signal(word.at[m, 1 - n], inc=1, device_id=to_x(d), device_id_type=MESH)
+
+    def hear(m):
+        for n in (0, 1):
+            pl.semaphore_wait(word.at[m, n], 1)
+
+    for n, d in ((1, 1), (2, nx - 1)):
+
+        @pl.when(jnp.logical_not(x_lower(d)))
+        def _():
+            pl.semaphore_wait(x_ready.at[n], 1)
+
+    tell(0)
+
     for copy in loads[6:]:
         copy.wait()
     row = lax.broadcasted_iota(jnp.int32, dw_v.shape, 0)
@@ -270,6 +288,9 @@
     @pl.when(z < HOP)
     def _():
         pass_on(0)
+
+    hear(0)
+    tell(1)
 
     total = part[z].astype(F32)
     arrived(near_in, near_recv, mate)
@@ -304,6 +325,9 @@
             to_z(sign[i] * k),
         )
         spread[i, k].start()
+    for m in range(1, nx // 2 - 2):
+        hear(m)
+        tell(m + 1)
     onward = {}
     for i in (0, 1):
         arrived(hid.at[0], hid_recv.at[i], mate)
@@ -374,12 +398,7 @@
         pl.semaphore_wait(x_ready.at[0], 1)
 
     multiply(0)
-    for d in range(1, nx):
-
-        @pl.when(jnp.logical_not(x_lower(d)))
-        def _():
-            pl.semaphore_wait(x_ready.at[d], 1)
-
+    hear(nx // 2 - 2)
     broadcast(0)
     multiply(1)
     broadcast(1)
@@ -457,7 +476,8 @@
                 pltpu.VMEM((2 * nz, 1, LANES), F32),
                 dma((11,)),
                 pltpu.SemaphoreType.REGULAR((2, HOP)),
-                pltpu.SemaphoreType.REGULAR((nx,)),
+                pltpu.SemaphoreType.REGULAR((3,)),
+                pltpu.SemaphoreType.REGULAR((nx // 2 - 1, 2)),
                 dma,
                 dma((2,)),
                 dma,

time: 84.9 us -> 83.8 us (0.987)
  Pallas kernels: 84.1 us -> 83.1 us
    pallas_call x1, Pallas kernels: 84.1 us -> 83.1 us  [on_device(): pl.pallas_call(functools.partial(kernel, nz, nc), out_shape=pltpu.VMEM((n...]
where the time goes in v6:
time: 83.8 us; the launch traced here: 83.7 us
  Pallas kernels  83.1 us (99%)
    pallas_call x1, Pallas kernels, on_device(): pl.pallas_call(functools.partial(kernel, nz, nc), out_shape=pltpu.VMEM((n...  83.1 us

profile of v6, /device:TPU:65, one launch (start us, length us, event | category | flops | bytes accessed | tf_op | source)
XLA Modules:
  0.0 83.7 jit_solution(10883189149360696718)
XLA Ops:
  0.0 83.1 %shard_map.91 = bf16[16,8,256]{2,1,0:T(8,128)(2,1)S(1)} custom-call(bf16[16,8,256]{2,1,0:T(8,128)(2,1)} %bitcast.10, f32[1,256]{1,0:T(1,128)} %bitcast.11, f32[704,256]{1,0:T(8,128)} %bitcast.8, f32[704]{0:T(1024)} %gs_hbm.1, f32[704,256]{1,0:T(8,128)} %bitcast.9, f32[704]{0:T(1024)} %us_hbm.1, f32[704,256]{1,0:T(8,128)} %dw_ref.1, f32[1,256]{1,0:T(1,128)} %bitcast.12, ...), custom_call_target="tpu_custom_call" | custom-call | tf_op jit(solution)/shard_map/pallas_call | solution.py:451
  83.1 0.6 copy.11

commit v7 on v6

--- a/solution.py
+++ b/solution.py
@@ -234,8 +234,6 @@
         def _():
             pl.semaphore_wait(ready.at[i, k - 1], 1)
             far[i, k].start()
-            if k < HOP:
-                near[i, k].start()
 
     def tell(m):
         for n, d in ((0, 1), (1, nx - 1)):
@@ -284,6 +282,13 @@
         pass_on(0)
 
     pass_on(1)
+
+    for i, k in rising:
+        if k < HOP:
+
+            @pl.when(jnp.logical_not(lower(i, k)))
+            def _():
+                near[i, k].start()
 
     @pl.when(z < HOP)
     def _():
@@ -313,32 +318,37 @@
     last = both * jax.nn.sigmoid(both) * swapped
     hid[HOP, :, main:] = jnp.where(tile_lane < rest, last, 0.0).astype(BF16)
 
-    hid_cols = hid.shape[2]
-    hid_halves = (slice(0, hid_cols // 2), slice(hid_cols // 2, hid_cols))
-    spread = {}
+    direct = nz // 2 - 1
+
+    def slot(d):
+        return (HOP - d) % nz
+
+    for d in (nz // 2, direct, -direct):
+        remote(hid.at[HOP], hid.at[slot(d)], hid_send, hid_recv.at[3], to_z(d)).start()
     for i, k in near_peers:
-        spread[i, k] = remote(
-            hid.at[HOP],
-            hid.at[(HOP - sign[i] * k) % nz],
-            hid_send,
-            hid_recv.at[i if k == HOP else 2],
-            to_z(sign[i] * k),
-        )
-        spread[i, k].start()
+        d = sign[i] * k
+        sem = hid_recv.at[i if k == HOP else 2]
+        remote(hid.at[HOP], hid.at[slot(d)], hid_send, sem, to_z(d)).start()
     for m in range(1, nx // 2 - 2):
         hear(m)
         tell(m + 1)
-    onward = {}
-    for i in (0, 1):
+
+    def forward(i):
         arrived(hid.at[0], hid_recv.at[i], mate)
-        for k in range(HOP, 0, -1):
-            src = hid.at[(HOP - sign[i] * HOP) % nz]
-            dst = hid.at[(HOP - sign[i] * (HOP + k)) % nz]
-            if k == HOP:
-                src = hid.at[(HOP - sign[i] * HOP) % nz, :, hid_halves[i]]
-                dst = hid.at[(HOP - sign[i] * (HOP + k)) % nz, :, hid_halves[i]]
-            onward[i, k] = remote(src, dst, hid_send, hid_recv.at[3], to_z(sign[i] * k))
-            onward[i, k].start()
+        src = hid.at[slot(sign[i] * HOP)]
+        for k in range(direct - HOP - 1, 0, -1):
+            dst = hid.at[slot(sign[i] * (HOP + k))]
+            remote(src, dst, hid_send, hid_recv.at[3], to_z(sign[i] * k)).start()
+
+    @pl.when(z >= nz // 2)
+    def _():
+        forward(0)
+
+    forward(1)
+
+    @pl.when(z < nz // 2)
+    def _():
+        forward(0)
 
     groups = 2
     size = nz // groups

time: 83.8 us -> 83.9 us (level)
  no operation moved by 1% of the time
where the time goes in v7:
time: 83.9 us; the launch traced here: 83.8 us
  Pallas kernels  83.1 us (99%)
    pallas_call x1, Pallas kernels, on_device(): pl.pallas_call(functools.partial(kernel, nz, nc), out_shape=pltpu.VMEM((n...  83.1 us

profile of v7, /device:TPU:65, one launch (start us, length us, event | category | flops | bytes accessed | tf_op | source)
XLA Modules:
  0.0 83.8 jit_solution(5009871527671176)
XLA Ops:
  0.0 83.1 %shard_map.91 = bf16[16,8,256]{2,1,0:T(8,128)(2,1)S(1)} custom-call(bf16[16,8,256]{2,1,0:T(8,128)(2,1)} %bitcast.10, f32[1,256]{1,0:T(1,128)} %bitcast.11, f32[704,256]{1,0:T(8,128)} %bitcast.8, f32[704]{0:T(1024)} %gs_hbm.1, f32[704,256]{1,0:T(8,128)} %bitcast.9, f32[704]{0:T(1024)} %us_hbm.1, f32[704,256]{1,0:T(8,128)} %dw_ref.1, f32[1,256]{1,0:T(1,128)} %bitcast.12, ...), custom_call_target="tpu_custom_call" | custom-call | tf_op jit(solution)/shard_map/pallas_call | solution.py:461
  83.2 0.6 copy.11

commit v8 on v7

--- a/solution.py
+++ b/solution.py
@@ -65,6 +65,9 @@
     near_in,
     relay_out,
     relay_in,
+    straight_in,
+    straight_half,
+    extra,
     hid,
     pair,
     pair_in,
@@ -75,6 +78,8 @@
     ready,
     x_ready,
     word,
+    late_ready,
+    straight_recv,
     rs_send,
     far_recv,
     near_recv,
@@ -122,6 +127,15 @@
     def lower(i, k):
         return block(sign[i] * k) < z
 
+    last = nz - 1
+    first, late = HOP - 1, nz - 1 - HOP
+
+    def at_z(index):
+        return {"ra": jnp.int32(index)}
+
+    def is_last(i, k):
+        return block(sign[i] * k) == last
+
     def turn(c):
         return jnp.minimum(c, nx - c) * nx + c
 
@@ -138,6 +152,15 @@
         @pl.when(jnp.logical_not(lower(i, k)))
         def _():
             pl.semaphore_signal(barrier, inc=1, device_id=to_z(sign[i] * k), device_id_type=MESH)
+
+    @pl.when(z == first)
+    def _():
+        for k in range(1, HOP + 1):
+            pl.semaphore_signal(barrier, inc=1, device_id=at_z(last - k), device_id_type=MESH)
+
+    @pl.when(z < first)
+    def _():
+        pl.semaphore_signal(barrier, inc=1, device_id=at_z(late), device_id_type=MESH)
 
     for d in beside:
 
@@ -168,6 +191,7 @@
 
     count = sum(jnp.where(lower(i, k), 1, 0) for i, k in near_peers)
     count += sum(jnp.where(x_lower(d), 1, 0) for d in beside)
+    count += jnp.where(z >= late, jnp.where(z < last, 1, 0), 0) + jnp.where(z == late, first, 0)
 
     @pl.when(count > 0)
     def _():
@@ -180,6 +204,11 @@
             pl.semaphore_signal(
                 ready.at[1 - i, k - 1], inc=1, device_id=to_z(sign[i] * k), device_id_type=MESH
             )
+
+    @pl.when(z == late)
+    def _():
+        for k in range(HOP):
+            pl.semaphore_signal(late_ready, inc=1, device_id=at_z(k), device_id_type=MESH)
 
     for n, d in enumerate(beside):
 
@@ -220,6 +249,20 @@
                 to_z(sign[i] * k),
             )
 
+    straight = {}
+    for i, k in near_peers:
+        src = part.at[block(sign[i] * (k + HOP))]
+        dst = straight_in.at[k - 1] if k < HOP else straight_half
+        if k == HOP:
+            src = part.at[block(sign[i] * (k + HOP)), :, halves[i]]
+        straight[i, k] = remote(src, dst, rs_send, straight_recv, to_z(sign[i] * (k + HOP)))
+
+    for k in range(HOP, 0, -1):
+
+        @pl.when(z == last - k)
+        def _():
+            straight[0, k].start()
+
     for table in (far, near):
         for i, k in near_peers:
             if (i, k) in table:
@@ -229,11 +272,23 @@
                     table[i, k].start()
 
     for i, k in rising:
+        if (i, k) == (1, HOP):
+            for j in range(HOP, 0, -1):
+
+                @pl.when(z == j - 1)
+                def _():
+                    pl.semaphore_wait(late_ready, 1)
+                    straight[1, j].start()
 
         @pl.when(jnp.logical_not(lower(i, k)))
         def _():
             pl.semaphore_wait(ready.at[i, k - 1], 1)
-            far[i, k].start()
+
+            @pl.when(jnp.logical_not(is_last(i, k)))
+            def _():
+                far[i, k].start()
+                if k < HOP:
+                    near[i, k].start()
 
     def tell(m):
         for n, d in ((0, 1), (1, nx - 1)):
@@ -263,19 +318,27 @@
     ]
 
     def pass_on(i):
-        arrived(part.at[: 2 * HOP - 1, :, halves[0]], far_recv.at[i], mate)
-        total = part[block(sign[i] * HOP)].astype(F32)
-        for k in range(1, HOP):
-            total += far_in[i, k - 1].astype(F32)
-        pieces = [total[:, halves[0]], total[:, halves[1]]]
-        pieces[i] += far_in_half[i].astype(F32)
-        last = pieces[1][:, -LANES:]
-        relay_out[i, :, halves[0]] = pieces[0].astype(BF16)
-        relay_out[i, :, cols // 2 : cols - LANES] = pieces[1][:, :-LANES].astype(BF16)
-        relay_out[i, :, cols - LANES :] = split_tail(
-            jnp.sum(last, axis=1, keepdims=True), tile_lane
-        ).astype(BF16)
-        relay[i].start()
+        @pl.when(z == last)
+        def _():
+            remote(
+                part.at[block(sign[i] * HOP)], relay_in.at[i], rs_send, relay_recv, to_z(sign[i] * HOP)
+            ).start()
+
+        @pl.when(z < last)
+        def _():
+            arrived(part.at[: 2 * HOP - 1, :, halves[0]], far_recv.at[i], mate)
+            total = part[block(sign[i] * HOP)].astype(F32)
+            for k in range(1, HOP):
+                total += far_in[i, k - 1].astype(F32)
+            pieces = [total[:, halves[0]], total[:, halves[1]]]
+            pieces[i] += far_in_half[i].astype(F32)
+            last = pieces[1][:, -LANES:]
+            relay_out[i, :, halves[0]] = pieces[0].astype(BF16)
+            relay_out[i, :, cols // 2 : cols - LANES] = pieces[1][:, :-LANES].astype(BF16)
+            relay_out[i, :, cols - LANES :] = split_tail(
+                jnp.sum(last, axis=1, keepdims=True), tile_lane
+            ).astype(BF16)
+            relay[i].start()
 
     @pl.when(z >= HOP)
     def _():
@@ -286,7 +349,7 @@
     for i, k in rising:
         if k < HOP:
 
-            @pl.when(jnp.logical_not(lower(i, k)))
+            @pl.when(is_last(i, k))
             def _():
                 near[i, k].start()
 
@@ -305,7 +368,20 @@
     gate_scale = gs_ref[...].reshape(1, units)
     up_scale = us_ref[...].reshape(1, units)
     mixed_scale = jnp.concatenate([gate_scale[:, main:], up_scale[:, main:]], axis=1)
+    extra[...] = jnp.zeros_like(extra)
+    for i, target in ((0, first), (1, late)):
+
+        @pl.when(z == target)
+        def _():
+            arrived(part.at[: 2 * HOP - 1, :, halves[0]], straight_recv, mate)
+            rest_of = straight_in[0].astype(F32)
+            for k in range(1, HOP - 1):
+                rest_of += straight_in[k].astype(F32)
+            extra[...] = rest_of
+            extra[:, halves[i]] += straight_half[...].astype(F32)
+
     arrived(relay_in, relay_recv, mate)
+    total += extra[...]
     for i in range(2):
         total += relay_in[i].astype(F32)
     square = jnp.sum(total[:, 2 * units :], axis=1, keepdims=True)
@@ -478,6 +554,9 @@
                 pltpu.VMEM((2, HOP - 1, tile, cols), BF16),
                 pltpu.VMEM((2, tile, cols), BF16),
                 pltpu.VMEM((2, tile, cols), BF16),
+                pltpu.VMEM((HOP - 1, tile, cols), BF16),
+                pltpu.VMEM((tile, cols // 2), BF16),
+                pltpu.VMEM((tile, cols), F32),
                 pltpu.VMEM((nz, tile, padded), BF16),
                 pltpu.VMEM((2, nz // 2, tile, feats), BF16),
                 pltpu.VMEM((2, share, tile, feats), BF16),
@@ -488,6 +567,8 @@
                 pltpu.SemaphoreType.REGULAR((2, HOP)),
                 pltpu.SemaphoreType.REGULAR((3,)),
                 pltpu.SemaphoreType.REGULAR((nx // 2 - 1, 2)),
+                pltpu.SemaphoreType.REGULAR,
+                dma,
                 dma,
                 dma((2,)),
                 dma,

time: 83.9 us -> 84.2 us (level)
  no operation moved by 1% of the time
where the time goes in v8:
time: 84.2 us; the launch traced here: 83.9 us
  Pallas kernels  83.3 us (99%)
    pallas_call x1, Pallas kernels, on_device(): pl.pallas_call(functools.partial(kernel, nz, nc), out_shape=pltpu.VMEM((n...  83.3 us

profile of v8, /device:TPU:65, one launch (start us, length us, event | category | flops | bytes accessed | tf_op | source)
XLA Modules:
  0.0 83.9 jit_solution(12983762242199543168)
XLA Ops:
  0.0 83.3 %shard_map.91 = bf16[16,8,256]{2,1,0:T(8,128)(2,1)S(1)} custom-call(bf16[16,8,256]{2,1,0:T(8,128)(2,1)} %bitcast.10, f32[1,256]{1,0:T(1,128)} %bitcast.11, f32[704,256]{1,0:T(8,128)} %bitcast.8, f32[704]{0:T(1024)} %gs_hbm.1, f32[704,256]{1,0:T(8,128)} %bitcast.9, f32[704]{0:T(1024)} %us_hbm.1, f32[704,256]{1,0:T(8,128)} %dw_ref.1, f32[1,256]{1,0:T(1,128)} %bitcast.12, ...), custom_call_target="tpu_custom_call" | custom-call | tf_op jit(solution)/shard_map/pallas_call | solution.py:537
  83.3 0.6 copy.11

commit v9 on v7

--- a/solution.py
+++ b/solution.py
@@ -80,6 +80,8 @@
     near_recv,
     relay_recv,
     hid_send,
+    late_send,
+    onward_send,
     hid_recv,
     pair_send,
     pair_recv,
@@ -122,6 +124,9 @@
     def lower(i, k):
         return block(sign[i] * k) < z
 
+    def is_last(i, k):
+        return block(sign[i] * k) == nz - 1
+
     def turn(c):
         return jnp.minimum(c, nx - c) * nx + c
 
@@ -234,6 +239,11 @@
         def _():
             pl.semaphore_wait(ready.at[i, k - 1], 1)
             far[i, k].start()
+            if k < HOP:
+
+                @pl.when(jnp.logical_not(is_last(i, k)))
+                def _():
+                    near[i, k].start()
 
     def tell(m):
         for n, d in ((0, 1), (1, nx - 1)):
@@ -286,7 +296,7 @@
     for i, k in rising:
         if k < HOP:
 
-            @pl.when(jnp.logical_not(lower(i, k)))
+            @pl.when(is_last(i, k))
             def _():
                 near[i, k].start()
 
@@ -329,16 +339,27 @@
         d = sign[i] * k
         sem = hid_recv.at[i if k == HOP else 2]
         remote(hid.at[HOP], hid.at[slot(d)], hid_send, sem, to_z(d)).start()
+    late = lax.rem(z, 2 * HOP) == HOP - 1
+    no_relay = lax.rem(z, 2 * HOP) == 2 * HOP - 1
+    between = [s * k for k in range(direct - 1, HOP, -1) for s in sign]
+
+    @pl.when(late)
+    def _():
+        for d in between:
+            remote(hid.at[HOP], hid.at[slot(d)], late_send, hid_recv.at[3], to_z(d)).start()
+
     for m in range(1, nx // 2 - 2):
         hear(m)
         tell(m + 1)
 
     def forward(i):
-        arrived(hid.at[0], hid_recv.at[i], mate)
-        src = hid.at[slot(sign[i] * HOP)]
-        for k in range(direct - HOP - 1, 0, -1):
-            dst = hid.at[slot(sign[i] * (HOP + k))]
-            remote(src, dst, hid_send, hid_recv.at[3], to_z(sign[i] * k)).start()
+        @pl.when(jnp.logical_not(no_relay))
+        def _():
+            arrived(hid.at[0], hid_recv.at[i], mate)
+            src = hid.at[slot(sign[i] * HOP)]
+            for k in range(direct - HOP - 1, 0, -1):
+                dst = hid.at[slot(sign[i] * (HOP + k))]
+                remote(src, dst, onward_send, hid_recv.at[3], to_z(sign[i] * k)).start()
 
     @pl.when(z >= nz // 2)
     def _():
@@ -356,6 +377,11 @@
 
     def multiply(k):
         arrived(hid.at[: 2 * HOP - 2 + k], hid_recv.at[2 + k], mate)
+
+        @pl.when(no_relay)
+        def _():
+            arrived(hid.at[0], hid_recv.at[k], mate)
+
         rows = hid[k * size : (k + 1) * size].reshape(size * tile, hid.shape[2])
         partial = jnp.dot(rows, down, preferred_element_type=F32)
         pair[k] = partial.reshape(size, tile, feats).astype(BF16)
@@ -436,7 +462,16 @@
         out_ref[block(r - HOP)] = result[r]
 
     left(part.at[: 4 * HOP - 1], rs_send, mate)
-    left(hid.at[: 4 * HOP - 1], hid_send, mate)
+    left(hid.at[: 2 * HOP + 3], hid_send, mate)
+
+    @pl.when(late)
+    def _():
+        left(hid.at[: len(between)], late_send, mate)
+
+    @pl.when(jnp.logical_not(no_relay))
+    def _():
+        left(hid.at[: len(between)], onward_send, mate)
+
     left(pair.at[0], pair_send, mate)
     left(chips.at[:, : nx - 1], chip_send, mate)
     left(mix.at[: 2 * share], mix_send, mate)
@@ -493,6 +528,8 @@
                 dma,
                 dma,
                 dma,
+                dma,
+                dma,
                 dma((4,)),
                 dma,
                 dma((2,)),

time: 83.9 us -> 84.1 us (level)
  no operation moved by 1% of the time
where the time goes in v9:
time: 84.1 us; the launch traced here: 84 us
  Pallas kernels  83.4 us (99%)
    pallas_call x1, Pallas kernels, on_device(): pl.pallas_call(functools.partial(kernel, nz, nc), out_shape=pltpu.VMEM((n...  83.4 us

profile of v9, /device:TPU:65, one launch (start us, length us, event | category | flops | bytes accessed | tf_op | source)
XLA Modules:
  0.0 84.0 jit_solution(1136383088454478363)
XLA Ops:
  0.0 83.4 %shard_map.91 = bf16[16,8,256]{2,1,0:T(8,128)(2,1)S(1)} custom-call(bf16[16,8,256]{2,1,0:T(8,128)(2,1)} %bitcast.10, f32[1,256]{1,0:T(1,128)} %bitcast.11, f32[704,256]{1,0:T(8,128)} %bitcast.8, f32[704]{0:T(1024)} %gs_hbm.1, f32[704,256]{1,0:T(8,128)} %bitcast.9, f32[704]{0:T(1024)} %us_hbm.1, f32[704,256]{1,0:T(8,128)} %dw_ref.1, f32[1,256]{1,0:T(1,128)} %bitcast.12, ...), custom_call_target="tpu_custom_call" | custom-call | tf_op jit(solution)/shard_map/pallas_call | solution.py:496
  83.4 0.6 copy.11

commit v10 on v7

--- a/solution.py
+++ b/solution.py
@@ -122,6 +122,9 @@
     def lower(i, k):
         return block(sign[i] * k) < z
 
+    def is_last(i, k):
+        return block(sign[i] * k) == nz - 1
+
     def turn(c):
         return jnp.minimum(c, nx - c) * nx + c
 
@@ -234,6 +237,11 @@
         def _():
             pl.semaphore_wait(ready.at[i, k - 1], 1)
             far[i, k].start()
+            if k < HOP:
+
+                @pl.when(jnp.logical_not(is_last(i, k)))
+                def _():
+                    near[i, k].start()
 
     def tell(m):
         for n, d in ((0, 1), (1, nx - 1)):
@@ -286,7 +294,7 @@
     for i, k in rising:
         if k < HOP:
 
-            @pl.when(jnp.logical_not(lower(i, k)))
+            @pl.when(is_last(i, k))
             def _():
                 near[i, k].start()
 
@@ -318,44 +326,23 @@
     last = both * jax.nn.sigmoid(both) * swapped
     hid[HOP, :, main:] = jnp.where(tile_lane < rest, last, 0.0).astype(BF16)
 
-    direct = nz // 2 - 1
-
     def slot(d):
         return (HOP - d) % nz
 
-    for d in (nz // 2, direct, -direct):
-        remote(hid.at[HOP], hid.at[slot(d)], hid_send, hid_recv.at[3], to_z(d)).start()
-    for i, k in near_peers:
-        d = sign[i] * k
-        sem = hid_recv.at[i if k == HOP else 2]
+    order = [nz // 2] + [s * k for k in range(nz // 2 - 1, 0, -1) for s in sign]
+    for d in order:
+        sem = hid_recv.at[0 if slot(d) < nz // 2 else 1]
         remote(hid.at[HOP], hid.at[slot(d)], hid_send, sem, to_z(d)).start()
     for m in range(1, nx // 2 - 2):
         hear(m)
         tell(m + 1)
 
-    def forward(i):
-        arrived(hid.at[0], hid_recv.at[i], mate)
-        src = hid.at[slot(sign[i] * HOP)]
-        for k in range(direct - HOP - 1, 0, -1):
-            dst = hid.at[slot(sign[i] * (HOP + k))]
-            remote(src, dst, hid_send, hid_recv.at[3], to_z(sign[i] * k)).start()
-
-    @pl.when(z >= nz // 2)
-    def _():
-        forward(0)
-
-    forward(1)
-
-    @pl.when(z < nz // 2)
-    def _():
-        forward(0)
-
     groups = 2
     size = nz // groups
     share = size // 2
 
     def multiply(k):
-        arrived(hid.at[: 2 * HOP - 2 + k], hid_recv.at[2 + k], mate)
+        arrived(hid.at[: size - 1 + k], hid_recv.at[k], mate)
         rows = hid[k * size : (k + 1) * size].reshape(size * tile, hid.shape[2])
         partial = jnp.dot(rows, down, preferred_element_type=F32)
         pair[k] = partial.reshape(size, tile, feats).astype(BF16)
@@ -436,7 +423,7 @@
         out_ref[block(r - HOP)] = result[r]
 
     left(part.at[: 4 * HOP - 1], rs_send, mate)
-    left(hid.at[: 4 * HOP - 1], hid_send, mate)
+    left(hid.at[: nz - 1], hid_send, mate)
     left(pair.at[0], pair_send, mate)
     left(chips.at[:, : nx - 1], chip_send, mate)
     left(mix.at[: 2 * share], mix_send, mate)
@@ -493,7 +480,7 @@
                 dma,
                 dma,
                 dma,
-                dma((4,)),
+                dma((2,)),
                 dma,
                 dma((2,)),
                 dma,

time: 83.9 us -> 84.5 us (level)
  no operation moved by 1% of the time
where the time goes in v10:
time: 84.5 us; the launch traced here: 84.4 us
  Pallas kernels  83.7 us (99%)
    pallas_call x1, Pallas kernels, on_device(): pl.pallas_call(functools.partial(kernel, nz, nc), out_shape=pltpu.VMEM((n...  83.7 us

profile of v10, /device:TPU:65, one launch (start us, length us, event | category | flops | bytes accessed | tf_op | source)
XLA Modules:
  0.0 84.4 jit_solution(8714403757543879703)
XLA Ops:
  0.0 83.7 %shard_map.91 = bf16[16,8,256]{2,1,0:T(8,128)(2,1)S(1)} custom-call(bf16[16,8,256]{2,1,0:T(8,128)(2,1)} %bitcast.10, f32[1,256]{1,0:T(1,128)} %bitcast.11, f32[704,256]{1,0:T(8,128)} %bitcast.8, f32[704]{0:T(1024)} %gs_hbm.1, f32[704,256]{1,0:T(8,128)} %bitcast.9, f32[704]{0:T(1024)} %us_hbm.1, f32[704,256]{1,0:T(8,128)} %dw_ref.1, f32[1,256]{1,0:T(1,128)} %bitcast.12, ...), custom_call_target="tpu_custom_call" | custom-call | tf_op jit(solution)/shard_map/pallas_call | solution.py:448
  83.7 0.6 copy.11

commit v11 on v10

--- a/solution.py
+++ b/solution.py
@@ -329,7 +329,9 @@
     def slot(d):
         return (HOP - d) % nz
 
-    order = [nz // 2] + [s * k for k in range(nz // 2 - 1, 0, -1) for s in sign]
+    most = nz // 2 - 1
+    steps = [most] + list(range(HOP, 0, -1)) + list(range(most - 1, HOP, -1))
+    order = [nz // 2] + [s * k for k in steps for s in sign]
     for d in order:
         sem = hid_recv.at[0 if slot(d) < nz // 2 else 1]
         remote(hid.at[HOP], hid.at[slot(d)], hid_send, sem, to_z(d)).start()

time: 84.5 us -> 84.2 us (level)
  no operation moved by 1% of the time
where the time goes in v11:
time: 84.2 us; the launch traced here: 84.1 us
  Pallas kernels  83.4 us (99%)
    pallas_call x1, Pallas kernels, on_device(): pl.pallas_call(functools.partial(kernel, nz, nc), out_shape=pltpu.VMEM((n...  83.4 us

profile of v11, /device:TPU:65, one launch (start us, length us, event | category | flops | bytes accessed | tf_op | source)
XLA Modules:
  0.0 84.1 jit_solution(14331288583813834179)
XLA Ops:
  0.0 83.4 %shard_map.91 = bf16[16,8,256]{2,1,0:T(8,128)(2,1)S(1)} custom-call(bf16[16,8,256]{2,1,0:T(8,128)(2,1)} %bitcast.10, f32[1,256]{1,0:T(1,128)} %bitcast.11, f32[704,256]{1,0:T(8,128)} %bitcast.8, f32[704]{0:T(1024)} %gs_hbm.1, f32[704,256]{1,0:T(8,128)} %bitcast.9, f32[704]{0:T(1024)} %us_hbm.1, f32[704,256]{1,0:T(8,128)} %dw_ref.1, f32[1,256]{1,0:T(1,128)} %bitcast.12, ...), custom_call_target="tpu_custom_call" | custom-call | tf_op jit(solution)/shard_map/pallas_call | solution.py:450
  83.4 0.6 copy.11

commit v12 on v7

--- a/solution.py
+++ b/solution.py
@@ -122,6 +122,9 @@
     def lower(i, k):
         return block(sign[i] * k) < z
 
+    def is_last(i, k):
+        return block(sign[i] * k) == nz - 1
+
     def turn(c):
         return jnp.minimum(c, nx - c) * nx + c
 
@@ -234,6 +237,11 @@
         def _():
             pl.semaphore_wait(ready.at[i, k - 1], 1)
             far[i, k].start()
+            if k < HOP:
+
+                @pl.when(jnp.logical_not(is_last(i, k)))
+                def _():
+                    near[i, k].start()
 
     def tell(m):
         for n, d in ((0, 1), (1, nx - 1)):
@@ -286,7 +294,7 @@
     for i, k in rising:
         if k < HOP:
 
-            @pl.when(jnp.logical_not(lower(i, k)))
+            @pl.when(is_last(i, k))
             def _():
                 near[i, k].start()
 

time: 83.9 us -> 84 us (level)
  no operation moved by 1% of the time
where the time goes in v12:
time: 84 us; the launch traced here: 83.9 us
  Pallas kernels  83.3 us (99%)
    pallas_call x1, Pallas kernels, on_device(): pl.pallas_call(functools.partial(kernel, nz, nc), out_shape=pltpu.VMEM((n...  83.3 us

profile of v12, /device:TPU:65, one launch (start us, length us, event | category | flops | bytes accessed | tf_op | source)
XLA Modules:
  0.0 83.9 jit_solution(9641368235065523178)
XLA Ops:
  0.0 83.3 %shard_map.91 = bf16[16,8,256]{2,1,0:T(8,128)(2,1)S(1)} custom-call(bf16[16,8,256]{2,1,0:T(8,128)(2,1)} %bitcast.10, f32[1,256]{1,0:T(1,128)} %bitcast.11, f32[704,256]{1,0:T(8,128)} %bitcast.8, f32[704]{0:T(1024)} %gs_hbm.1, f32[704,256]{1,0:T(8,128)} %bitcast.9, f32[704]{0:T(1024)} %us_hbm.1, f32[704,256]{1,0:T(8,128)} %dw_ref.1, f32[1,256]{1,0:T(1,128)} %bitcast.12, ...), custom_call_target="tpu_custom_call" | custom-call | tf_op jit(solution)/shard_map/pallas_call | solution.py:469
  83.3 0.6 copy.11

commit v13 on v7

--- a/solution.py
+++ b/solution.py
@@ -234,6 +234,8 @@
         def _():
             pl.semaphore_wait(ready.at[i, k - 1], 1)
             far[i, k].start()
+            if k < HOP:
+                near[i, k].start()
 
     def tell(m):
         for n, d in ((0, 1), (1, nx - 1)):
@@ -282,13 +284,6 @@
         pass_on(0)
 
     pass_on(1)
-
-    for i, k in rising:
-        if k < HOP:
-
-            @pl.when(jnp.logical_not(lower(i, k)))
-            def _():
-                near[i, k].start()
 
     @pl.when(z < HOP)
     def _():

time: 83.9 us -> 85 us (1.013)
  Pallas kernels: 83.1 us -> 84.2 us
    pallas_call x1, Pallas kernels: 83.1 us -> 84.2 us  [on_device(): pl.pallas_call(functools.partial(kernel, nz, nc), out_shape=pltpu.VMEM((n...]
where the time goes in v13:
time: 85 us; the launch traced here: 84.8 us
  Pallas kernels  84.2 us (99%)
    pallas_call x1, Pallas kernels, on_device(): pl.pallas_call(functools.partial(kernel, nz, nc), out_shape=pltpu.VMEM((n...  84.2 us

profile of v13, /device:TPU:65, one launch (start us, length us, event | category | flops | bytes accessed | tf_op | source)
XLA Modules:
  0.0 84.8 jit_solution(18262612110500465846)
XLA Ops:
  0.0 84.2 %shard_map.91 = bf16[16,8,256]{2,1,0:T(8,128)(2,1)S(1)} custom-call(bf16[16,8,256]{2,1,0:T(8,128)(2,1)} %bitcast.10, f32[1,256]{1,0:T(1,128)} %bitcast.11, f32[704,256]{1,0:T(8,128)} %bitcast.8, f32[704]{0:T(1024)} %gs_hbm.1, f32[704,256]{1,0:T(8,128)} %bitcast.9, f32[704]{0:T(1024)} %us_hbm.1, f32[704,256]{1,0:T(8,128)} %dw_ref.1, f32[1,256]{1,0:T(1,128)} %bitcast.12, ...), custom_call_target="tpu_custom_call" | custom-call | tf_op jit(solution)/shard_map/pallas_call | solution.py:456
  84.2 0.6 copy.11
